TPU v7x, 32 devices: a whole 2x2x4 slice. The times are simulated.
32 devices in a mesh: sp: 4 (over z), fs: 4 (over y, x), tp: 2 (over core).
Axes of the slice: x: 2, y: 2, z: 4, core: 2. Of those that a mesh axis runs over, the one named last changes fastest.
Arguments:
- activations: bfloat16 [2048, 4096], P(('fs', 'sp'), 'tp'), parts along dimension 0, may hold values from -6 to 6
- input_norm_gain: float32 [4096], replicated, may hold values from 0.1 to 1.9
- window_query_weight: bfloat16 [4096, 2048], P('sp', 'tp'), may hold values from -0.09375 to 0.09375
- window_key_weight: bfloat16 [4096, 512], P('sp', 'tp'), may hold values from -0.09375 to 0.09375
- window_value_weight: bfloat16 [4096, 512], P('sp', 'tp'), may hold values from -0.09375 to 0.09375
- linear_query_weight: bfloat16 [4096, 1024], P('sp', 'tp'), may hold values from -0.09375 to 0.09375
- linear_key_weight: bfloat16 [4096, 1024], P('sp', 'tp'), may hold values from -0.09375 to 0.09375
- linear_value_weight: bfloat16 [4096, 2048], P('sp', 'tp'), may hold values from -0.09375 to 0.09375
- decay_down_factor: bfloat16 [4096, 16], replicated, may hold values from -0.09375 to 0.09375
- decay_up_factor: bfloat16 [16, 1024], P(None, 'tp'), may hold values from -1.5 to 1.5
- decay_offset_bias: float32 [1024], P('tp'), may hold values from -0.5 to 9
- extra_fading_exponent: float32 [2048, 8], P(('fs', 'sp'), 'tp'), parts along dimension 0, may hold values from -1.5 to 0
- starting_state: float32 [8, 128, 256], P('tp'), may hold values from -12 to 12
- head_sink_logit: float32 [32], P('tp'), may hold values from 1 to 5
- linear_head_gain: float32 [256], replicated, may hold values from 0.1 to 1.9
- window_output_weight: bfloat16 [2048, 4096], P('tp', 'sp'), may hold values from -0.09375 to 0.09375
- linear_output_weight: bfloat16 [2048, 4096], P('tp', 'sp'), may hold values from -0.09375 to 0.09375
Outputs:
- mixer_output: bfloat16 [2048, 4096], P(('fs', 'sp', 'tp')), parts along dimension 0
There are 4 independent parts, one for each index of `fs`. A program takes and returns all parts, laid end to end along the dimension named above; an argument that names none is the same for every part. Nothing has to cross between parts.
All inputs are finite; a program needn't handle non-finite values.
Results may differ from a plain program's by a relative error of at most 0.019.
Values may be sent and summed in bfloat16 or wider, within the bound.
A program may use at most 128 MiB of HBM per device.

v0:
```python
import functools

import jax
import jax.numpy as jnp
from jax import lax
from jax.experimental import pallas as pl
from jax.experimental.pallas import tpu as pltpu
from jax.sharding import PartitionSpec as P

QH = 32
HD = 64
WINDOW = 128
LOOKUP_FEATURES = 128
DV = 256
SPAN = 64
KVH = 8
GATED_MIXERS = 8


EPS = 1e-05
FADING_SOFTNESS = 16.0
HIGH_PRECISION = lax.Precision.HIGHEST


def passed_along(value, axis, steps):
    count = lax.axis_size(axis)
    leading, last = (max(0, -steps), min(count, count - steps))
    return lax.ppermute(value, axis, [(source, source + steps) for source in range(leading, last)])


def prefix(x, axis, combine, identity):
    peers, place = (lax.axis_size(axis), lax.axis_index(axis))
    everything = jax.tree.map(
        lambda part, kind: lax.all_gather(part.astype(kind), axis), x, (jnp.bfloat16, jnp.bfloat16)
    )
    start = jax.tree.map(
        lambda part, zero: jnp.broadcast_to(jnp.asarray(zero, part.dtype), part.shape), x, identity
    )

    def hop(k, before):
        reached = k < place
        new = combine(
            before, jax.tree.map(lambda part, own: part[k].astype(own.dtype), everything, x)
        )
        return jax.tree.map(lambda a, b: jnp.where(reached, a, b), new, before)

    return lax.fori_loop(0, peers, hop, start)


def window_attention(near_query, near_keys, near_values, head_sink_logit):
    stream_extent = near_query.shape[0]
    key_heads = near_keys.shape[1] // HD
    heads_here = near_query.shape[1] // HD
    groups = heads_here // key_heads
    blocks = stream_extent // WINDOW
    tail_rows = jnp.stack([near_keys, near_values])
    before = passed_along(tail_rows, "sp", 1)

    def banded(previous, current):
        extended = jnp.concatenate([previous, current], axis=0)
        earlier = extended[:stream_extent].reshape(blocks, WINDOW, key_heads, HD)
        present = extended[WINDOW:].reshape(blocks, WINDOW, key_heads, HD)
        return jnp.concatenate([earlier, present], axis=1)

    key_band = banded(before[0], near_keys)
    value_band = banded(before[1], near_values)
    queries = near_query.reshape(blocks, WINDOW, key_heads, groups, HD)
    scores = jnp.einsum(
        "nqhgd,nkhd->hgnqk", queries, key_band, preferred_element_type=jnp.float32
    ) * HD ** (-0.5)
    head_ids = lax.axis_index("tp") * heads_here + jnp.arange(heads_here, dtype=jnp.int32)
    slopes = jnp.exp2(-8.0 * (head_ids + 1).astype(jnp.float32) / QH).reshape(key_heads, groups)
    query_pos = jnp.arange(WINDOW, dtype=jnp.int32)
    key_pos = jnp.arange(2 * WINDOW, dtype=jnp.int32)
    distance = query_pos[:, None] - key_pos[None, :] + WINDOW
    start_pos = (
        lax.axis_index("sp") * stream_extent + (jnp.arange(blocks, dtype=jnp.int32) - 1) * WINDOW
    )
    absolute = start_pos[:, None] + key_pos[None, :]
    allowed = ((distance >= 0) & (distance < WINDOW))[None] & (absolute >= 0)[:, None, :]
    biased = scores - slopes[:, :, None, None, None] * distance.astype(jnp.float32)
    weights = jnp.where(allowed, jnp.exp(biased), 0.0)
    denominator = (
        jnp.sum(weights, axis=-1, keepdims=True)
        + jnp.exp(head_sink_logit.reshape(key_heads, groups))[:, :, None, None, None]
    )
    attention = (weights / denominator).astype(jnp.bfloat16)
    attended = jnp.einsum(
        "hgnqk,nkhd->nqhgd", attention, value_band, preferred_element_type=jnp.float32
    )
    return attended.reshape(stream_extent, heads_here * HD).astype(jnp.bfloat16)


def linear_attention(
    gated_query, gated_keys, gated_values, fading_exponent, linear_head_gain, starting_state
):
    stream_extent = gated_query.shape[0]
    head_total = gated_query.shape[1] // LOOKUP_FEATURES
    span_count = stream_extent // SPAN
    scaled_query = gated_query.astype(jnp.float32).reshape(
        span_count, SPAN, head_total, LOOKUP_FEATURES
    ) * LOOKUP_FEATURES ** (-0.5)
    keys_wide = gated_keys.astype(jnp.float32).reshape(
        span_count, SPAN, head_total, LOOKUP_FEATURES
    )
    values_wide = gated_values.astype(jnp.float32).reshape(span_count, SPAN, head_total, DV)
    running = jnp.cumsum(
        fading_exponent.reshape(span_count, SPAN, head_total, LOOKUP_FEATURES), axis=1
    )
    span_end = running[:, -1]
    query_with_decay = scaled_query * jnp.exp(running)
    inverse_keys = keys_wide * jnp.exp(-running)
    ending_keys = keys_wide * jnp.exp(span_end[:, None] - running)
    inner = jnp.einsum("nchk,nshk->nhcs", query_with_decay, inverse_keys, precision=HIGH_PRECISION)
    lower = jnp.tril(jnp.ones((SPAN, SPAN), dtype=bool))
    inner = jnp.where(lower, inner, 0.0)
    within = jnp.einsum("nhcs,nshv->nchv", inner, values_wide, precision=HIGH_PRECISION)

    def advance(running_state, inputs):
        query_portion, key_portion, value_portion, scale_factor = inputs
        layer_output = jnp.einsum(
            "fmy,mys->fms", query_portion, running_state, precision=HIGH_PRECISION
        )
        running_state = running_state * scale_factor[..., None] + jnp.einsum(
            "gxp,gxz->xpz", key_portion, value_portion, precision=HIGH_PRECISION
        )
        return (running_state, layer_output)

    start_state = jnp.zeros((head_total, LOOKUP_FEATURES, DV), jnp.float32)
    state_end, carried = lax.scan(
        advance, start_state, (query_with_decay, ending_keys, values_wide, jnp.exp(span_end))
    )
    device_decay = jnp.exp(jnp.sum(span_end, axis=0))
    prefix_sums = jnp.cumsum(span_end, axis=0) - span_end

    def combine(earlier, later):
        return (earlier[0] * later[0], later[0][..., None] * earlier[1] + later[1])

    decay_before, state_before = prefix(
        (device_decay, state_end),
        "sp",
        combine,
        (jnp.ones_like(device_decay), jnp.zeros_like(state_end)),
    )
    incoming_rows = state_before + decay_before[..., None] * starting_state
    crossing = jnp.einsum(
        "qwso,soz->qwsz",
        query_with_decay * jnp.exp(prefix_sums)[:, None],
        incoming_rows,
        precision=HIGH_PRECISION,
    )
    flat = (within + carried + crossing).reshape(stream_extent, head_total, DV)
    normal = (
        flat * lax.rsqrt(jnp.mean(flat * flat, axis=-1, keepdims=True) + EPS) * linear_head_gain
    )
    return normal.reshape(stream_extent, head_total * DV).astype(jnp.bfloat16)


def local(
    activations,
    input_norm_gain,
    window_query_weight,
    window_key_weight,
    window_value_weight,
    linear_query_weight,
    linear_key_weight,
    linear_value_weight,
    decay_down_factor,
    decay_up_factor,
    decay_offset_bias,
    extra_fading_exponent,
    starting_state,
    head_sink_logit,
    linear_head_gain,
    window_output_weight,
    linear_output_weight,
):
    gathered = lax.all_gather(activations, "tp", axis=1, tiled=True)
    widened = gathered.astype(jnp.float32)
    normed = (
        widened
        * lax.rsqrt(jnp.mean(widened * widened, axis=1, keepdims=True) + EPS)
        * input_norm_gain
    ).astype(jnp.bfloat16)
    row_total = normed.shape[0]
    matrices = (
        window_query_weight,
        window_key_weight,
        window_value_weight,
        linear_query_weight,
        linear_key_weight,
        linear_value_weight,
    )
    segments = (
        lax.all_gather(matrices[0], "sp", axis=0, tiled=True),
        lax.all_gather(matrices[1], "sp", axis=0, tiled=True),
        lax.all_gather(matrices[2], "sp", axis=0, tiled=True),
        lax.all_gather(matrices[3], "sp", axis=0, tiled=True),
        lax.all_gather(matrices[4], "sp", axis=0, tiled=True),
        lax.all_gather(matrices[5], "sp", axis=0, tiled=True),
    )
    projected = tuple(
        (jnp.dot(normed, segment, preferred_element_type=jnp.float32) for segment in segments)
    )
    near_query, near_keys, near_values, gated_query, gated_keys, gated_values = [
        product.astype(jnp.bfloat16) for product in projected
    ]
    low_rank = jnp.dot(normed, decay_down_factor, preferred_element_type=jnp.float32).astype(
        jnp.bfloat16
    )
    attention_energies = (
        jnp.dot(low_rank, decay_up_factor, preferred_element_type=jnp.float32) + decay_offset_bias
    )
    head_total = extra_fading_exponent.shape[1]
    fading_exponent = (jax.nn.log_sigmoid(attention_energies) / FADING_SOFTNESS).reshape(
        row_total, head_total, LOOKUP_FEATURES
    ) + extra_fading_exponent[:, :, None]
    near_out = window_attention(near_query, near_keys, near_values, head_sink_logit)
    gated_out = linear_attention(
        gated_query, gated_keys, gated_values, fading_exponent, linear_head_gain, starting_state
    )
    window_full, linear_full = (
        lax.all_gather(window_output_weight, "sp", axis=1, tiled=True),
        lax.all_gather(linear_output_weight, "sp", axis=1, tiled=True),
    )
    return lax.psum_scatter(
        (
            jnp.dot(near_out, window_full, preferred_element_type=jnp.float32)
            + jnp.dot(gated_out, linear_full, preferred_element_type=jnp.float32)
        ).astype(jnp.bfloat16),
        "tp",
        scatter_dimension=0,
        tiled=True,
    )


MESH = pl.DeviceIdType.MESH
BF = jnp.bfloat16
F32 = jnp.float32


def dot(a, b):
    return jnp.dot(a, b, preferred_element_type=F32)


def remote(src, dst, send_sem, recv_sem, **where):
    return pltpu.make_async_remote_copy(
        src_ref=src,
        dst_ref=dst,
        send_sem=send_sem,
        recv_sem=recv_sem,
        device_id=where,
        device_id_type=MESH,
    )


def greet(sp, tp):
    s, t = lax.axis_index("sp"), lax.axis_index("tp")
    barrier = pltpu.get_barrier_semaphore()
    for ds in range(sp):
        for dt in range(tp):
            if ds or dt:
                where = {"sp": lax.rem(s + ds, sp), "tp": lax.rem(t + dt, tp)}
                pl.semaphore_signal(barrier, inc=1, device_id=where, device_id_type=MESH)
    pl.semaphore_wait(barrier, sp * tp - 1)


def columns_dot(a, b):
    return lax.dot_general(a, b, (((1,), (1,)), ((), ())), preferred_element_type=F32)


def mixer_kernel(sp, tp, widths, order, *refs):
    x, gain, down, fade, up, bias, sink, head_gain = refs[:8]
    sources, state_in, out = refs[8:16], refs[16], refs[17]
    weights, start = refs[18:26], refs[26]
    squares, normed, blocks, note, term, away, landed = refs[27:34]
    lin = refs[34:38]
    held_g, held_n = refs[38:40]
    w_sem, sq_sem, a_send, a_recv, f_send, l_sem, n_send, n_recv = refs[40:48]
    lin_sem, g_sem, h_sem = refs[48:52], refs[52:56], refs[56:60]
    t_send, t_recv, o_send, o_recv = refs[60:64]
    s, t = lax.axis_index("sp"), lax.axis_index("tp")
    other = 1 - t
    after, ahead = jnp.minimum(s + 1, sp - 1), jnp.maximum(s - 1, 0)
    per_half = sp // tp
    rows, half = x.shape
    width = half // per_half
    rank = down.shape[1]
    loads = [
        pltpu.make_async_copy(a, b, w_sem.at[i]) for i, (a, b) in enumerate(zip(sources, weights))
    ]
    loads.append(pltpu.make_async_copy(state_in.at[s], start, w_sem.at[len(sources)]))
    for i in (3, 4, 5, 0, 1, 2, 8, 6, 7):
        loads[i].start()
    wide = x[...].astype(F32)
    own = jnp.sum(wide * wide, axis=1, keepdims=True)
    squares[0] = jnp.broadcast_to(own, (rows, 128))
    greet(sp, tp)
    swap_squares = remote(squares.at[0], squares.at[1], sq_sem.at[0], sq_sem.at[1], tp=other)
    swap_squares.start()
    swap_squares.wait()
    total = own + squares[1][:, :1]
    scale = lax.rsqrt(total / (half * tp) + EPS)
    home = lax.div(s, per_half) == t

    def slice_send(i):
        j = t * per_half + i
        return remote(normed.at[i], blocks.at[s], a_send.at[i], a_recv.at[s], sp=j)

    for i in range(per_half):
        cols = slice(i * width, (i + 1) * width)
        normed[i] = (x[:, cols].astype(F32) * scale * gain[t, :, cols]).astype(BF)

        @pl.when(t * per_half + i != s)
        def _():
            slice_send(i).start()

        @pl.when(t * per_half + i == s)
        def _():
            keep = pltpu.make_async_copy(normed.at[i], blocks.at[s], l_sem)
            keep.start()
            keep.wait()

    def forward(b):
        return remote(blocks.at[b], blocks.at[b], f_send.at[b], a_recv.at[b], tp=other)

    @pl.when(home)
    def _():
        forward(s).start()

    low = jnp.zeros((rank, rows), F32)
    for i in range(per_half):
        low += columns_dot(down[t, :, i * width : (i + 1) * width], normed[i])
    note[s, t, :rank] = low
    note[s, t, rank:] = fade[...]

    def note_send(n):
        where = {"sp": lax.rem(s + n // tp, sp), "tp": lax.rem(t + n % tp, tp)}
        return remote(note.at[s, t], note.at[s, t], n_send.at[n], n_recv.at[s, t], **where)

    def right(group, sems, b, d):
        return remote(group[0].at[b, d], group[1].at[b, d], sems[0].at[b, d], sems[1].at[b, d], sp=after)

    def left(group, sems, b, d):
        return remote(group[0].at[b, d], group[2].at[b, d], sems[2].at[b, d], sems[3].at[b, d], sp=ahead)

    def ends(group, sems, k):
        for n in range(2):

            @pl.when(jnp.logical_and(s == 0, k == 0))
            def _():
                right(group, sems, 0, sp - 1 - n).start()

            @pl.when(jnp.logical_and(s == sp - 1, k == 0))
            def _():
                left(group, sems, sp - 1, n).start()

    def paced(group, sems, k, n):
        ready = k >= 0 if n > 1 else k >= 1
        k_old, n_old = (k, n - 2) if n > 1 else (k - 1, n + sp - 3)

        @pl.when(jnp.logical_and(s == 0, ready))
        def _():
            right(group, sems, k_old, sp - 1 - n_old).wait_send()
            right(group, sems, k, sp - 1 - n).start()

        @pl.when(jnp.logical_and(s == sp - 1, ready))
        def _():
            left(group, sems, sp - 1 - k_old, n_old).wait_send()
            left(group, sems, sp - 1 - k, n).start()

    def place(k):
        return lax.rem(s + jnp.where(s < (sp + 1) // 2, k, sp - k), sp)

    for i in range(6):
        loads[i].wait()

    def project(k, carry):
        b = place(k)

        @pl.when(jnp.logical_or(jnp.logical_not(home), b != s))
        def _():
            forward(b).wait_recv()

        @pl.when(jnp.logical_and(home, b != s))
        def _():
            forward(b).start()

        block = blocks[b]
        keys = dot(block, weights[1][...])
        vals = dot(block, weights[2][...])
        kw, vw = widths[1], widths[2]
        for d in range(sp):
            at = 0
            for i in (3, 4, 5, 0):
                w = widths[i]
                lin[0][b, d, :, at : at + w] = dot(block, weights[i][:, d * w : (d + 1) * w]).astype(BF)
                at += w
            lin[0][b, d, :, at : at + kw] = keys[:, d * kw : (d + 1) * kw].astype(BF)
            lin[0][b, d, :, at + kw :] = vals[:, d * vw : (d + 1) * vw].astype(BF)
        ends(lin, lin_sem, k)
        return carry

    lax.fori_loop(0, sp, project, 0)
    for n in range(1, sp * tp):
        note_send(n).start()

    def relay(group, sems, k):
        br, bl = k, sp - 1 - k
        for n in range(sp - 1):
            dr, dl = sp - 1 - n, n
            paced(group, sems, k, n)

            @pl.when(jnp.logical_and(s > 0, s < dr))
            def _():
                right(group, sems, br, dr).wait_recv()
                group[0][br, dr] = (
                    group[0][br, dr].astype(F32) + group[1][br, dr].astype(F32)
                ).astype(BF)
                right(group, sems, br, dr).start()

            @pl.when(jnp.logical_and(s < sp - 1, s > dl))
            def _():
                left(group, sems, bl, dl).wait_recv()
                group[0][bl, dl] = (
                    group[0][bl, dl].astype(F32) + group[2][bl, dl].astype(F32)
                ).astype(BF)
                left(group, sems, bl, dl).start()

    def relay_step(k, carry):
        relay(lin, lin_sem, k)
        return carry

    lax.fori_loop(0, sp, relay_step, 0)

    def finish(group, sems, b):
        group[3][b] = group[0][b, s]

        @pl.when(s > 0)
        def _():
            right(group, sems, b, s).wait_recv()
            group[3][b] = (group[3][b].astype(F32) + group[1][b, s].astype(F32)).astype(BF)

        @pl.when(s < sp - 1)
        def _():
            left(group, sems, b, s).wait_recv()
            group[3][b] = (group[3][b].astype(F32) + group[2][b, s].astype(F32)).astype(BF)

    def sent(group, sems, b):
        for d in range(sp):
            last_right = jnp.logical_or(s > 0, jnp.logical_and(b == sp - 1, d <= 2))
            last_left = jnp.logical_or(s < sp - 1, jnp.logical_and(b == 0, d >= sp - 3))

            @pl.when(jnp.logical_and(s < d, last_right))
            def _():
                right(group, sems, b, d).wait_send()

            @pl.when(jnp.logical_and(s > d, last_left))
            def _():
                left(group, sems, b, d).wait_send()

    def gather_right(held, sems, b, src):
        ref = held.at[b, src]
        return remote(ref, ref, sems[0].at[b, src], sems[1].at[b, src], sp=after)

    def gather_left(held, sems, b, src):
        ref = held.at[b, src]
        return remote(ref, ref, sems[2].at[b, src], sems[3].at[b, src], sp=ahead)

    def start_own(held, sems, b):
        @pl.when(s < sp - 1)
        def _():
            gather_right(held, sems, b, s).start()

        @pl.when(s > 0)
        def _():
            gather_left(held, sems, b, s).start()

    def pass_on(held, sems, b):
        for n in range(1, sp):

            @pl.when(s - n >= 0)
            def _():
                src = jnp.maximum(s - n, 0)
                gather_right(held, sems, b, src).wait_recv()

                @pl.when(s < sp - 1)
                def _():
                    gather_right(held, sems, b, src).start()

            @pl.when(s + n < sp)
            def _():
                src = jnp.minimum(s + n, sp - 1)
                gather_left(held, sems, b, src).wait_recv()

                @pl.when(s > 0)
                def _():
                    gather_left(held, sems, b, src).start()

    loads[8].wait()
    for n in range(1, sp * tp):
        ps, pt = lax.rem(s + n // tp, sp), lax.rem(t + n % tp, tp)
        remote(note.at[ps, pt], note.at[ps, pt], n_send.at[n], n_recv.at[ps, pt], tp=other).wait_recv()
    lk = LOOKUP_FEATURES
    lane = pl.ds(pl.multiple_of(s * lk, lk), lk)
    up_own = jnp.concatenate([up[:, lane], jnp.zeros((rows - rank, lk), BF)], axis=0)
    bias_own = bias[:, lane]
    row_at = lax.broadcasted_iota(jnp.int32, (rows, rows), 0)
    col_at = lax.broadcasted_iota(jnp.int32, (rows, rows), 1)
    span_low = jnp.logical_and(row_at >= col_at, row_at // SPAN == col_at // SPAN)
    ones_low = jnp.where(span_low, 1.0, 0.0)
    noted = note.shape[2]
    wide = sum(widths[3:])

    def linear(b, state):
        finish(lin, lin_sem, b)
        rank_rows = note[b, 0, :rank] + note[b, 1, :rank]
        tall = jnp.concatenate(
            [rank_rows, note[b, t, rank:], jnp.zeros((rows - noted, rows), F32)], axis=0
        ).T
        energies = dot(tall.astype(BF), up_own) + bias_own
        soft = jnp.minimum(energies, 0.0) - jnp.log1p(jnp.exp(-jnp.abs(energies)))
        extra = jnp.sum(jnp.where(col_at == rank + s, tall, 0.0), axis=1, keepdims=True)
        fading = soft / FADING_SOFTNESS + extra
        running = lax.dot_general(
            ones_low,
            fading,
            (((1,), (0,)), ((), ())),
            precision=HIGH_PRECISION,
            preferred_element_type=F32,
        )
        query = lin[3][b, :, :lk].astype(F32) * lk ** (-0.5)
        key = lin[3][b, :, lk : 2 * lk].astype(F32)
        value = lin[3][b, :, 2 * lk : wide]
        decayed = (query * jnp.exp(running)).astype(BF)
        inner = columns_dot(decayed, (key * jnp.exp(-running)).astype(BF))
        inner = jnp.where(span_low, inner, 0.0).astype(BF)
        within = dot(inner, value)
        carried = []
        for j in range(rows // SPAN):
            cut = slice(j * SPAN, (j + 1) * SPAN)
            end = running[(j + 1) * SPAN - 1 : (j + 1) * SPAN]
            ending = (key[cut] * jnp.exp(end - running[cut])).astype(BF)
            carried.append(columns_dot(decayed[cut], state.astype(BF)))
            state = state * jnp.exp(end) + lax.dot_general(
                value[cut], ending, (((0,), (0,)), ((), ())), preferred_element_type=F32
            )
        flat = within + jnp.concatenate(carried, axis=0)
        normal = flat * lax.rsqrt(jnp.mean(flat * flat, axis=-1, keepdims=True) + EPS) * head_gain[...]
        q, r = divmod(order.index(b), 2)
        held_g[q, s, r * rows : (r + 1) * rows] = normal.astype(BF)
        return state

    state = start[...].T
    for b in range(sp):
        state = linear(b, state)
    for q in range(sp // 2):
        start_own(held_g, g_sem, q)

    query_at = lax.broadcasted_iota(jnp.int32, (rows, 2 * rows), 0)
    key_at = lax.broadcasted_iota(jnp.int32, (rows, 2 * rows), 1)
    distance = query_at - key_at + rows
    near_by = jnp.logical_and(distance >= 0, distance < WINDOW)
    far = distance.astype(F32)
    heads = widths[0] // HD
    qw = widths[0]
    for b in order:
        present = lin[3][b, :, wide:]
        earlier = lin[3][max(b - 1, 0), :, wide:]
        keys = jnp.concatenate([earlier[:, qw : qw + HD], present[:, qw : qw + HD]], axis=0)
        vals = jnp.concatenate([earlier[:, qw + HD :], present[:, qw + HD :]], axis=0)
        allowed = near_by if b else jnp.logical_and(near_by, key_at >= rows)
        results = []
        for h in range(heads):
            number = ((t * sp + s) * heads + h + 1).astype(F32)
            slope = jnp.exp2(jnp.full((rows, 1), -8.0 / QH, F32) * number)
            score = columns_dot(present[:, h * HD : (h + 1) * HD], keys) * HD ** (-0.5) - slope * far
            weight = jnp.where(allowed, jnp.exp(score), 0.0)
            floor = jnp.exp(jnp.full((rows, 1), sink[s * heads + h], F32))
            probs = (weight / (jnp.sum(weight, axis=1, keepdims=True) + floor)).astype(BF)
            results.append(dot(probs, vals))
        q, r = divmod(order.index(b), 2)
        held_n[q, s, r * rows : (r + 1) * rows] = jnp.concatenate(results, axis=1).astype(BF)
        if r:
            start_own(held_n, h_sem, q)

    loads[6].wait()
    loads[7].wait()
    part = rows // tp
    near_cols, gated_cols = held_n.shape[3], held_g.shape[3]

    def swap(b):
        return remote(term.at[b, other], away.at[b], t_send.at[b], t_recv.at[b], tp=other)

    def deliver(b):
        return remote(term.at[b, t], landed.at[s], o_send.at[b], o_recv.at[s], sp=b)

    def close(b):
        swap(b).wait()
        term[b, t] = (term[b, t].astype(F32) + away[b].astype(F32)).astype(BF)

        @pl.when(s != b)
        def _():
            deliver(b).start()

        @pl.when(s == b)
        def _():
            landed[b] = term[b, t]

    for q in range(sp // 2):
        pass_on(held_g, g_sem, q)
    for k, b in enumerate(order):
        q, r = divmod(k, 2)
        if r == 0:
            pass_on(held_n, h_sem, q)
        if k:
            close(order[k - 1])
        total = None
        for src in range(sp):
            piece = dot(held_n[q, src, r * rows : (r + 1) * rows], weights[6][src * near_cols : (src + 1) * near_cols]) + dot(
                held_g[q, src, r * rows : (r + 1) * rows], weights[7][src * gated_cols : (src + 1) * gated_cols]
            )
            total = piece if total is None else total + piece
        for h in range(tp):
            term[b, h] = total[h * part : (h + 1) * part].astype(BF)
        swap(b).start()
    close(order[-1])

    def drain(b, carry):
        sent(lin, lin_sem, b)

        @pl.when(home)
        def _():
            forward(b).wait_send()

        return carry

    lax.fori_loop(0, sp, drain, 0)
    for held, sems in ((held_g, g_sem), (held_n, h_sem)):
        for q in range(sp // 2):
            for src in range(sp):

                @pl.when(jnp.logical_and(src <= s, s < sp - 1))
                def _():
                    gather_right(held, sems, q, src).wait_send()

                @pl.when(jnp.logical_and(src >= s, s > 0))
                def _():
                    gather_left(held, sems, q, src).wait_send()

    for i in range(per_half):

        @pl.when(t * per_half + i != s)
        def _():
            slice_send(i).wait_send()

    for n in range(1, sp * tp):
        note_send(n).wait_send()
    columns = landed.shape[2]
    for b in range(sp):

        @pl.when(s != b)
        def _():
            deliver(b).wait_send()
            remote(landed.at[b], landed.at[b], o_send.at[b], o_recv.at[b], tp=other).wait_recv()

        out[:, b * columns : (b + 1) * columns] = landed[b]


def stationary(
    activations,
    input_norm_gain,
    window_query_weight,
    window_key_weight,
    window_value_weight,
    linear_query_weight,
    linear_key_weight,
    linear_value_weight,
    decay_down_factor,
    decay_up_factor,
    decay_offset_bias,
    extra_fading_exponent,
    starting_state,
    head_sink_logit,
    linear_head_gain,
    window_output_weight,
    linear_output_weight,
):
    sp, tp = lax.axis_size("sp"), lax.axis_size("tp")
    rows, half = activations.shape
    matrices = (
        window_query_weight,
        window_key_weight,
        window_value_weight,
        linear_query_weight,
        linear_key_weight,
        linear_value_weight,
        window_output_weight,
        linear_output_weight,
    )
    widths = tuple(m.shape[1] // sp for m in matrices[:6])
    rank = decay_down_factor.shape[1]
    heads_tp = extra_fading_exponent.shape[1]
    gain = input_norm_gain.reshape(tp, 1, half)
    down = decay_down_factor.T.reshape(rank, tp, half).transpose(1, 0, 2)
    fade = jnp.pad(extra_fading_exponent.T, ((0, -heads_tp % 8), (0, 0)))
    noted = rank + fade.shape[0]
    columns = window_output_weight.shape[1]
    order = sorted(range(sp), key=lambda b: -abs(2 * b - sp + 1))
    vmem = pl.BlockSpec(memory_space=pltpu.VMEM)
    hbm = pl.BlockSpec(memory_space=pltpu.HBM)
    dma = pltpu.SemaphoreType.DMA
    slice_width = half * tp // sp

    def chunks(cols):
        return [pltpu.VMEM((sp, sp, rows, cols), BF)] * 3 + [pltpu.VMEM((sp, rows, cols), BF)]

    return pl.pallas_call(
        functools.partial(mixer_kernel, sp, tp, widths, order),
        out_shape=jax.ShapeDtypeStruct((rows // tp, columns * sp), BF),
        in_specs=[vmem] * 6
        + [pl.BlockSpec(memory_space=pltpu.SMEM), vmem]
        + [hbm] * 9,
        out_specs=vmem,
        scratch_shapes=[pltpu.VMEM(m.shape, BF) for m in matrices]
        + [
            pltpu.VMEM(starting_state.shape[1:], F32),
            pltpu.VMEM((2, rows, 128), F32),
            pltpu.VMEM((sp // tp, rows, slice_width), BF),
            pltpu.VMEM((sp, rows, slice_width), BF),
            pltpu.VMEM((sp, tp, noted, rows), F32),
            pltpu.VMEM((sp, tp, rows // tp, columns), BF),
            pltpu.VMEM((sp, rows // tp, columns), BF),
            pltpu.VMEM((sp, rows // tp, columns), BF),
        ]
        + chunks(sum(widths))
        + [
            pltpu.VMEM((sp // 2, sp, 2 * rows, widths[5]), BF),
            pltpu.VMEM((sp // 2, sp, 2 * rows, widths[0]), BF),
            dma((9,)),
            dma((2,)),
            dma((sp // tp,)),
            dma((sp,)),
            dma((sp,)),
            dma,
            dma((sp * tp,)),
            dma((sp, tp)),
        ]
        + [dma((sp, sp))] * 12
        + [dma((sp,))] * 4,
        compiler_params=pltpu.CompilerParams(
            collective_id=0, has_side_effects=True, vmem_limit_bytes=56 * 2**20
        ),
    )(
        activations,
        gain,
        down,
        fade,
        decay_up_factor,
        decay_offset_bias.reshape(1, -1),
        head_sink_logit,
        linear_head_gain.reshape(1, -1),
        *matrices,
        starting_state,
    )


def mixer(*arrays):
    sp, tp = lax.axis_size("sp"), lax.axis_size("tp")
    rows = arrays[0].shape[0]
    one_each = KVH == GATED_MIXERS == sp * tp and QH % KVH == 0
    if tp == 2 and sp % tp == 0 and one_each and rows == WINDOW and rows % SPAN == 0:
        return stationary(*arrays)
    return local(*arrays)


def solution(mesh):
    placed = (
        P(("fs", "sp"), "tp"),
        P(),
        P("sp", "tp"),
        P("sp", "tp"),
        P("sp", "tp"),
        P("sp", "tp"),
        P("sp", "tp"),
        P("sp", "tp"),
        P(),
        P(None, "tp"),
        P("tp"),
        P(("fs", "sp"), "tp"),
        P("tp", None, None),
        P("tp"),
        P(),
        P("tp", "sp"),
        P("tp", "sp"),
    )
    return jax.shard_map(
        mixer, mesh=mesh, in_specs=placed, out_specs=P(("fs", "sp", "tp"), None), check_vma=False
    )
```

profile of v0, /device:TPU:0, one launch (start us, length us, event | category | flops | bytes accessed | tf_op | source)
XLA Modules:
  0.0 153.2 jit_solution(1297336828763055876)
XLA Ops:
  0.0 1.3 pad.4.refs_3_
  1.3 1.6 %copy.21 = bf16[2,2,8,2048]{3,2,0,1:T(8,128)(2,1)} copy(bf16[2,2,8,2048]{3,2,1,0:T(8,128)(2,1)} %bitcast.13) | data formatting | bytes 262144 | tf_op jit(solution)/shard_map/reshape | solution.py:705
  2.8 148.5 %shard_map.163 = bf16[64,4096]{1,0:T(8,128)(2,1)} custom-call(bf16[128,2048]{1,0:T(8,128)(2,1)} %refs_0_.1, f32[2,1,2048]{2,1,0:T(1,128)} %bitcast.14, bf16[2,16,2048]{2,1,0:T(8,128)(2,1)} %bitcast.12, f32[8,128]{1,0:T(8,128)} %pad.4.refs_3_, bf16[16,512]{1,0:T(8,128)(2,1)} %refs_4_.1, f32[1,512]{1,0:T(1,128)} %bitcast.16, f32[16]{0:T(128)} %refs_6_.1, ...), custom_call_target="tpu_custom_call" | custom-call | tf_op jit(solution)/shard_map/pallas_call | solution.py:718
  151.4 1.9 %copy.23 = bf16[64,4096]{1,0:T(8,128)(2,1)} copy(bf16[64,4096]{1,0:T(8,128)(2,1)} %shard_map.163) | data formatting | bytes 1048576
where the time goes:
time: 153 us
  Pallas kernels  149 us (97%)
  local copies, waits for them, and re-layouts  4.71 us (3%)
    pallas_call x1, Pallas kernels, stationary(): pl.pallas_call(functools.partial(mixer_kernel, sp, tp, widths, order), ou...  149 us

commit v1 on v0

v1 whole, which is shorter than its diff:
```python
import functools

import jax
import jax.numpy as jnp
from jax import lax
from jax.experimental import pallas as pl
from jax.experimental.pallas import tpu as pltpu
from jax.sharding import PartitionSpec as P

QH = 32
HD = 64
WINDOW = 128
LOOKUP_FEATURES = 128
DV = 256
SPAN = 64
KVH = 8
GATED_MIXERS = 8


EPS = 1e-05
FADING_SOFTNESS = 16.0
HIGH_PRECISION = lax.Precision.HIGHEST


def passed_along(value, axis, steps):
    count = lax.axis_size(axis)
    leading, last = (max(0, -steps), min(count, count - steps))
    return lax.ppermute(value, axis, [(source, source + steps) for source in range(leading, last)])


def prefix(x, axis, combine, identity):
    peers, place = (lax.axis_size(axis), lax.axis_index(axis))
    everything = jax.tree.map(
        lambda part, kind: lax.all_gather(part.astype(kind), axis), x, (jnp.bfloat16, jnp.bfloat16)
    )
    start = jax.tree.map(
        lambda part, zero: jnp.broadcast_to(jnp.asarray(zero, part.dtype), part.shape), x, identity
    )

    def hop(k, before):
        reached = k < place
        new = combine(
            before, jax.tree.map(lambda part, own: part[k].astype(own.dtype), everything, x)
        )
        return jax.tree.map(lambda a, b: jnp.where(reached, a, b), new, before)

    return lax.fori_loop(0, peers, hop, start)


def window_attention(near_query, near_keys, near_values, head_sink_logit):
    stream_extent = near_query.shape[0]
    key_heads = near_keys.shape[1] // HD
    heads_here = near_query.shape[1] // HD
    groups = heads_here // key_heads
    blocks = stream_extent // WINDOW
    tail_rows = jnp.stack([near_keys, near_values])
    before = passed_along(tail_rows, "sp", 1)

    def banded(previous, current):
        extended = jnp.concatenate([previous, current], axis=0)
        earlier = extended[:stream_extent].reshape(blocks, WINDOW, key_heads, HD)
        present = extended[WINDOW:].reshape(blocks, WINDOW, key_heads, HD)
        return jnp.concatenate([earlier, present], axis=1)

    key_band = banded(before[0], near_keys)
    value_band = banded(before[1], near_values)
    queries = near_query.reshape(blocks, WINDOW, key_heads, groups, HD)
    scores = jnp.einsum(
        "nqhgd,nkhd->hgnqk", queries, key_band, preferred_element_type=jnp.float32
    ) * HD ** (-0.5)
    head_ids = lax.axis_index("tp") * heads_here + jnp.arange(heads_here, dtype=jnp.int32)
    slopes = jnp.exp2(-8.0 * (head_ids + 1).astype(jnp.float32) / QH).reshape(key_heads, groups)
    query_pos = jnp.arange(WINDOW, dtype=jnp.int32)
    key_pos = jnp.arange(2 * WINDOW, dtype=jnp.int32)
    distance = query_pos[:, None] - key_pos[None, :] + WINDOW
    start_pos = (
        lax.axis_index("sp") * stream_extent + (jnp.arange(blocks, dtype=jnp.int32) - 1) * WINDOW
    )
    absolute = start_pos[:, None] + key_pos[None, :]
    allowed = ((distance >= 0) & (distance < WINDOW))[None] & (absolute >= 0)[:, None, :]
    biased = scores - slopes[:, :, None, None, None] * distance.astype(jnp.float32)
    weights = jnp.where(allowed, jnp.exp(biased), 0.0)
    denominator = (
        jnp.sum(weights, axis=-1, keepdims=True)
        + jnp.exp(head_sink_logit.reshape(key_heads, groups))[:, :, None, None, None]
    )
    attention = (weights / denominator).astype(jnp.bfloat16)
    attended = jnp.einsum(
        "hgnqk,nkhd->nqhgd", attention, value_band, preferred_element_type=jnp.float32
    )
    return attended.reshape(stream_extent, heads_here * HD).astype(jnp.bfloat16)


def linear_attention(
    gated_query, gated_keys, gated_values, fading_exponent, linear_head_gain, starting_state
):
    stream_extent = gated_query.shape[0]
    head_total = gated_query.shape[1] // LOOKUP_FEATURES
    span_count = stream_extent // SPAN
    scaled_query = gated_query.astype(jnp.float32).reshape(
        span_count, SPAN, head_total, LOOKUP_FEATURES
    ) * LOOKUP_FEATURES ** (-0.5)
    keys_wide = gated_keys.astype(jnp.float32).reshape(
        span_count, SPAN, head_total, LOOKUP_FEATURES
    )
    values_wide = gated_values.astype(jnp.float32).reshape(span_count, SPAN, head_total, DV)
    running = jnp.cumsum(
        fading_exponent.reshape(span_count, SPAN, head_total, LOOKUP_FEATURES), axis=1
    )
    span_end = running[:, -1]
    query_with_decay = scaled_query * jnp.exp(running)
    inverse_keys = keys_wide * jnp.exp(-running)
    ending_keys = keys_wide * jnp.exp(span_end[:, None] - running)
    inner = jnp.einsum("nchk,nshk->nhcs", query_with_decay, inverse_keys, precision=HIGH_PRECISION)
    lower = jnp.tril(jnp.ones((SPAN, SPAN), dtype=bool))
    inner = jnp.where(lower, inner, 0.0)
    within = jnp.einsum("nhcs,nshv->nchv", inner, values_wide, precision=HIGH_PRECISION)

    def advance(running_state, inputs):
        query_portion, key_portion, value_portion, scale_factor = inputs
        layer_output = jnp.einsum(
            "fmy,mys->fms", query_portion, running_state, precision=HIGH_PRECISION
        )
        running_state = running_state * scale_factor[..., None] + jnp.einsum(
            "gxp,gxz->xpz", key_portion, value_portion, precision=HIGH_PRECISION
        )
        return (running_state, layer_output)

    start_state = jnp.zeros((head_total, LOOKUP_FEATURES, DV), jnp.float32)
    state_end, carried = lax.scan(
        advance, start_state, (query_with_decay, ending_keys, values_wide, jnp.exp(span_end))
    )
    device_decay = jnp.exp(jnp.sum(span_end, axis=0))
    prefix_sums = jnp.cumsum(span_end, axis=0) - span_end

    def combine(earlier, later):
        return (earlier[0] * later[0], later[0][..., None] * earlier[1] + later[1])

    decay_before, state_before = prefix(
        (device_decay, state_end),
        "sp",
        combine,
        (jnp.ones_like(device_decay), jnp.zeros_like(state_end)),
    )
    incoming_rows = state_before + decay_before[..., None] * starting_state
    crossing = jnp.einsum(
        "qwso,soz->qwsz",
        query_with_decay * jnp.exp(prefix_sums)[:, None],
        incoming_rows,
        precision=HIGH_PRECISION,
    )
    flat = (within + carried + crossing).reshape(stream_extent, head_total, DV)
    normal = (
        flat * lax.rsqrt(jnp.mean(flat * flat, axis=-1, keepdims=True) + EPS) * linear_head_gain
    )
    return normal.reshape(stream_extent, head_total * DV).astype(jnp.bfloat16)


def local(
    activations,
    input_norm_gain,
    window_query_weight,
    window_key_weight,
    window_value_weight,
    linear_query_weight,
    linear_key_weight,
    linear_value_weight,
    decay_down_factor,
    decay_up_factor,
    decay_offset_bias,
    extra_fading_exponent,
    starting_state,
    head_sink_logit,
    linear_head_gain,
    window_output_weight,
    linear_output_weight,
):
    gathered = lax.all_gather(activations, "tp", axis=1, tiled=True)
    widened = gathered.astype(jnp.float32)
    normed = (
        widened
        * lax.rsqrt(jnp.mean(widened * widened, axis=1, keepdims=True) + EPS)
        * input_norm_gain
    ).astype(jnp.bfloat16)
    row_total = normed.shape[0]
    matrices = (
        window_query_weight,
        window_key_weight,
        window_value_weight,
        linear_query_weight,
        linear_key_weight,
        linear_value_weight,
    )
    segments = (
        lax.all_gather(matrices[0], "sp", axis=0, tiled=True),
        lax.all_gather(matrices[1], "sp", axis=0, tiled=True),
        lax.all_gather(matrices[2], "sp", axis=0, tiled=True),
        lax.all_gather(matrices[3], "sp", axis=0, tiled=True),
        lax.all_gather(matrices[4], "sp", axis=0, tiled=True),
        lax.all_gather(matrices[5], "sp", axis=0, tiled=True),
    )
    projected = tuple(
        (jnp.dot(normed, segment, preferred_element_type=jnp.float32) for segment in segments)
    )
    near_query, near_keys, near_values, gated_query, gated_keys, gated_values = [
        product.astype(jnp.bfloat16) for product in projected
    ]
    low_rank = jnp.dot(normed, decay_down_factor, preferred_element_type=jnp.float32).astype(
        jnp.bfloat16
    )
    attention_energies = (
        jnp.dot(low_rank, decay_up_factor, preferred_element_type=jnp.float32) + decay_offset_bias
    )
    head_total = extra_fading_exponent.shape[1]
    fading_exponent = (jax.nn.log_sigmoid(attention_energies) / FADING_SOFTNESS).reshape(
        row_total, head_total, LOOKUP_FEATURES
    ) + extra_fading_exponent[:, :, None]
    near_out = window_attention(near_query, near_keys, near_values, head_sink_logit)
    gated_out = linear_attention(
        gated_query, gated_keys, gated_values, fading_exponent, linear_head_gain, starting_state
    )
    window_full, linear_full = (
        lax.all_gather(window_output_weight, "sp", axis=1, tiled=True),
        lax.all_gather(linear_output_weight, "sp", axis=1, tiled=True),
    )
    return lax.psum_scatter(
        (
            jnp.dot(near_out, window_full, preferred_element_type=jnp.float32)
            + jnp.dot(gated_out, linear_full, preferred_element_type=jnp.float32)
        ).astype(jnp.bfloat16),
        "tp",
        scatter_dimension=0,
        tiled=True,
    )


MESH = pl.DeviceIdType.MESH
BF = jnp.bfloat16
F32 = jnp.float32


def dot(a, b):
    return jnp.dot(a, b, preferred_element_type=F32)


def remote(src, dst, send_sem, recv_sem, **where):
    return pltpu.make_async_remote_copy(
        src_ref=src,
        dst_ref=dst,
        send_sem=send_sem,
        recv_sem=recv_sem,
        device_id=where,
        device_id_type=MESH,
    )


def greet(sp, tp):
    s, t = lax.axis_index("sp"), lax.axis_index("tp")
    barrier = pltpu.get_barrier_semaphore()
    for ds in range(sp):
        for dt in range(tp):
            if ds or dt:
                where = {"sp": lax.rem(s + ds, sp), "tp": lax.rem(t + dt, tp)}
                pl.semaphore_signal(barrier, inc=1, device_id=where, device_id_type=MESH)
    pl.semaphore_wait(barrier, sp * tp - 1)


def columns_dot(a, b):
    return lax.dot_general(a, b, (((1,), (1,)), ((), ())), preferred_element_type=F32)


def mixer_kernel(sp, tp, *refs):
    x, gain, bias, sink, head_gain, up, fade = refs[:7]
    sources, state_in, down_in, out = refs[7:15], refs[15], refs[16], refs[17]
    weights, start, down = refs[18:26], refs[26], refs[27]
    squares, normed, blocks, note, term, away, landed = refs[28:35]
    lin_own, win_own, lin_in, win_in, held_g, held_n = refs[35:41]
    w_sem, sq_sem, a_send, a_recv, f_send, l_sem, n_send, n_recv = refs[41:49]
    r_send, r_recv, g_send, g_recv, t_send, t_recv, o_send, o_recv, y_sem = refs[49:58]
    s, t = lax.axis_index("sp"), lax.axis_index("tp")
    other = 1 - t
    last = sp - 1
    e = jnp.where(s >= sp // 2, 1, 0)
    at_end = jnp.logical_or(s == 0, s == last)
    inside = jnp.logical_not(at_end)
    per_half = sp // tp
    rows, half = x.shape
    width = half // per_half
    rank = down.shape[1]
    lk = LOOKUP_FEATURES
    mine = lin_own.shape[2]
    lane_of = {i: weights[i].shape[1] // 2 for i in range(6)}
    loads = [
        pltpu.make_async_copy(a, b, w_sem.at[i]) for i, (a, b) in enumerate(zip(sources, weights))
    ]
    loads.append(pltpu.make_async_copy(state_in.at[pl.ds(e * mine, mine)], start, w_sem.at[8]))
    loads.append(
        pltpu.make_async_copy(
            down_in.at[pl.ds(pl.multiple_of(t * half, half), half)], down, w_sem.at[9]
        )
    )
    for i in (9, 3, 4, 5, 0, 1, 2, 8, 6, 7):
        loads[i].start()
    wide = x[...].astype(F32)
    own = jnp.sum(wide * wide, axis=1, keepdims=True)
    squares[0] = jnp.broadcast_to(own, (rows, 128))
    greet(sp, tp)
    swap_squares = remote(squares.at[0], squares.at[1], sq_sem.at[0], sq_sem.at[1], tp=other)
    swap_squares.start()
    swap_squares.wait()
    total = own + squares[1][:, :1]
    scale = lax.rsqrt(total / (half * tp) + EPS)
    home = lax.div(s, per_half) == t

    def slice_send(i):
        j = t * per_half + i
        return remote(normed.at[i], blocks.at[s], a_send.at[i], a_recv.at[s], sp=j)

    for i in range(per_half):
        cols = slice(i * width, (i + 1) * width)
        normed[i] = (x[:, cols].astype(F32) * scale * gain[t, :, cols]).astype(BF)

        @pl.when(t * per_half + i != s)
        def _():
            slice_send(i).start()

        @pl.when(t * per_half + i == s)
        def _():
            keep = pltpu.make_async_copy(normed.at[i], blocks.at[s], l_sem)
            keep.start()
            keep.wait()

    def forward(b):
        return remote(blocks.at[b], blocks.at[b], f_send.at[b], a_recv.at[b], tp=other)

    @pl.when(home)
    def _():
        forward(s).start()

    loads[9].wait()
    low = jnp.zeros((rows, rank), F32)
    for i in range(per_half):
        low += dot(normed[i], down[i * width : (i + 1) * width])
    fades = fade.shape[1]
    noted = note.shape[2]
    wide_note = jnp.concatenate(
        [low, fade[...], jnp.zeros((rows, rows - rank - fades), F32)], axis=1
    )
    note[s, t] = wide_note.T[:noted]

    def note_send(n):
        place, core = (0 if n < tp else last), lax.rem(t + n % tp, tp)
        ref = note.at[s, t]
        return remote(ref, ref, n_send.at[n], n_recv.at[s, t], sp=place, tp=core), jnp.logical_or(
            s != place, core != t
        )

    for n in range(2 * tp):
        send, away_from_here = note_send(n)

        @pl.when(away_from_here)
        def _():
            send.start()

    def step(way, b, i):
        src = lin_own.at[b, 1 - way, i] if i < mine else win_own.at[b, 1 - way]
        dst = lin_in.at[way, b, i] if i < mine else win_in.at[way, b]
        return remote(
            src, dst, r_send.at[way, b, i], r_recv.at[way, b, i], sp=jnp.clip(s + 1 - 2 * way, 0, last)
        )

    def relay(way, b):
        for i in range(mine + 1):
            step(way, b, i).wait_recv()
            if i < mine:
                lin_own[b, 1 - way, i] = (
                    lin_own[b, 1 - way, i].astype(F32) + lin_in[way, b, i].astype(F32)
                ).astype(BF)
            else:
                win_own[b, 1 - way] = (
                    win_own[b, 1 - way].astype(F32) + win_in[way, b].astype(F32)
                ).astype(BF)
            step(way, b, i).start()

    for i in range(6):
        loads[i].wait()
    qw, kw = lane_of[0], lane_of[1]

    def project(b, carry):
        @pl.when(jnp.logical_or(jnp.logical_not(home), b != s))
        def _():
            forward(b).wait_recv()

        @pl.when(jnp.logical_and(home, b != s))
        def _():
            forward(b).start()

        block = blocks[b]

        def part(i, h):
            w = lane_of[i]
            return dot(block, weights[i][:, pl.ds(pl.multiple_of(h * w, w), w)]).astype(BF)

        for n in range(2):
            h = e if n else 1 - e
            query, key, value = part(3, h), part(4, h), part(5, h)
            for i in range(mine):
                lin_own[b, h, i, :, :lk] = query[:, i * lk : (i + 1) * lk]
                lin_own[b, h, i, :, lk : 2 * lk] = key[:, i * lk : (i + 1) * lk]
                lin_own[b, h, i, :, 2 * lk :] = value[:, i * DV : (i + 1) * DV]
            if n == 0:

                @pl.when(at_end)
                def _():
                    for i in range(mine):
                        step(e, b, i).start()

            win_own[b, h, :, :qw] = part(0, h)
            win_own[b, h, :, qw : qw + kw] = part(1, h)
            win_own[b, h, :, qw + kw :] = part(2, h)
            if n == 0:

                @pl.when(at_end)
                def _():
                    step(e, b, mine).start()

        @pl.when(jnp.logical_and(inside, b >= 1))
        def _():
            relay(0, b - 1)

        @pl.when(jnp.logical_and(inside, b >= 2))
        def _():
            relay(1, b - 2)

        return carry

    lax.fori_loop(0, sp, project, 0)

    def gather(way, b, i):
        ref = (held_g if i == 0 else held_n).at[b, way]
        return remote(
            ref, ref, g_send.at[way, b, i], g_recv.at[way, b, i], sp=jnp.clip(s + 1 - 2 * way, 0, last)
        )

    part_rows = rows // tp
    cols_g, cols_n = held_g.shape[3], held_n.shape[3]

    def swap(b):
        return remote(term.at[b, other], away.at[b], t_send.at[b], t_recv.at[b], tp=other)

    def deliver(b):
        return remote(term.at[b, t], landed.at[s], o_send.at[b], o_recv.at[s], sp=b)

    def close(b):
        swap(b).wait()
        term[b, t] = (term[b, t].astype(F32) + away[b].astype(F32)).astype(BF)

        @pl.when(s != b)
        def _():
            deliver(b).start()

        @pl.when(s == b)
        def _():
            landed[b] = term[b, t]

    def multiply(b):
        total = None
        for src in range(2):
            piece = dot(held_g[b, src], weights[7][src * cols_g : (src + 1) * cols_g]) + dot(
                held_n[b, src], weights[6][src * cols_n : (src + 1) * cols_n]
            )
            total = piece if total is None else total + piece
        for h in range(tp):
            term[b, h] = total[h * part_rows : (h + 1) * part_rows].astype(BF)
        swap(b).start()

    def pass_on(b):
        for i in range(2):
            for way in range(2):
                gather(way, b, i).wait_recv()
                gather(way, b, i).start()

    @pl.when(inside)
    def _():
        loads[8].wait()
        relay(1, sp - 2)
        pass_on(0)
        relay(0, last)
        relay(1, last)
        pass_on(1)
        loads[6].wait()
        loads[7].wait()
        for b in range(sp):
            multiply(b)
            if b + 2 < sp:
                pass_on(b + 2)
            if b:
                close(b - 1)
        close(last)

    @pl.when(at_end)
    def _():
        loads[8].wait()
        for ps in range(sp):
            for pt in range(tp):

                @pl.when(jnp.logical_or(s != ps, t != pt))
                def _():
                    ref = note.at[ps, pt]
                    remote(ref, ref, n_send.at[0], n_recv.at[ps, pt], tp=other).wait_recv()

        span = mine * lk
        lane = pl.ds(pl.multiple_of(e * span, span), span)
        up_own = jnp.concatenate([up[:, lane], jnp.zeros((rows - rank, span), BF)], axis=0)
        bias_own = bias[:, lane]
        row_at = lax.broadcasted_iota(jnp.int32, (rows, rows), 0)
        col_at = lax.broadcasted_iota(jnp.int32, (rows, rows), 1)
        span_low = jnp.logical_and(row_at >= col_at, row_at // SPAN == col_at // SPAN)
        ones_low = jnp.where(span_low, 1.0, 0.0).astype(BF)
        query_at = lax.broadcasted_iota(jnp.int32, (rows, 2 * rows), 0)
        key_at = lax.broadcasted_iota(jnp.int32, (rows, 2 * rows), 1)
        distance = query_at - key_at + rows
        near_by = jnp.logical_and(distance >= 0, distance < WINDOW)
        far = distance.astype(F32)
        heads = qw // HD // mine

        def linear(b, states):
            rank_rows = note[b, 0, :rank] + note[b, 1, :rank]
            tall = jnp.concatenate(
                [rank_rows, note[b, t, rank:], jnp.zeros((rows - noted, rows), F32)], axis=0
            ).T
            energies = dot(tall.astype(BF), up_own) + bias_own
            soft = jnp.minimum(energies, 0.0) - jnp.log1p(jnp.exp(-jnp.abs(energies)))
            soft = soft / FADING_SOFTNESS
            fading = []
            for i in range(mine):
                extra = jnp.sum(
                    jnp.where(col_at == rank + e * mine + i, tall, 0.0), axis=1, keepdims=True
                )
                fading.append(soft[:, i * lk : (i + 1) * lk] + extra)
            fading = jnp.concatenate(fading, axis=1)
            top = fading.astype(BF)
            rest = fading - top.astype(F32)
            middle = rest.astype(BF)
            bottom = (rest - middle.astype(F32)).astype(BF)
            summed = dot(ones_low, jnp.concatenate([top, middle, bottom], axis=1))
            running_all = summed[:, :span] + (summed[:, span : 2 * span] + summed[:, 2 * span :])
            new_states = []
            for i in range(mine):
                step(1 - e, b, i).wait_recv()
                here = (lin_own[b, e, i].astype(F32) + lin_in[1 - e, b, i].astype(F32)).astype(BF)
                running = running_all[:, i * lk : (i + 1) * lk]
                state = states[i]
                query = here[:, :lk].astype(F32) * lk ** (-0.5)
                key = here[:, lk : 2 * lk].astype(F32)
                value = here[:, 2 * lk :]
                decayed = (query * jnp.exp(running)).astype(BF)
                inner = columns_dot(decayed, (key * jnp.exp(-running)).astype(BF))
                inner = jnp.where(span_low, inner, 0.0).astype(BF)
                within = dot(inner, value)
                carried = []
                for j in range(rows // SPAN):
                    cut = slice(j * SPAN, (j + 1) * SPAN)
                    end = running[(j + 1) * SPAN - 1 : (j + 1) * SPAN]
                    ending = (key[cut] * jnp.exp(end - running[cut])).astype(BF)
                    carried.append(columns_dot(decayed[cut], state.astype(BF)))
                    state = state * jnp.exp(end) + lax.dot_general(
                        value[cut], ending, (((0,), (0,)), ((), ())), preferred_element_type=F32
                    )
                flat = within + jnp.concatenate(carried, axis=0)
                normal = (
                    flat
                    * lax.rsqrt(jnp.mean(flat * flat, axis=-1, keepdims=True) + EPS)
                    * head_gain[...]
                )
                held_g[b, e, :, i * DV : (i + 1) * DV] = normal.astype(BF)
                new_states.append(state)
            gather(e, b, 0).start()
            return new_states

        def window(b):
            step(1 - e, b, mine).wait_recv()
            win_own[b, e] = (win_own[b, e].astype(F32) + win_in[1 - e, b].astype(F32)).astype(BF)
            present = win_own[b, e]
            earlier = win_own[max(b - 1, 0), e]
            allowed = near_by if b else jnp.logical_and(near_by, key_at >= rows)
            for g in range(mine):
                ka, va = qw + g * HD, qw + kw + g * HD
                keys = jnp.concatenate([earlier[:, ka : ka + HD], present[:, ka : ka + HD]], axis=0)
                vals = jnp.concatenate([earlier[:, va : va + HD], present[:, va : va + HD]], axis=0)
                results = []
                for h in range(heads):
                    local = (e * mine + g) * heads + h
                    number = (t * (2 * mine * heads) + local + 1).astype(F32)
                    slope = jnp.exp2(jnp.full((rows, 1), -8.0 / QH, F32) * number)
                    at = (g * heads + h) * HD
                    score = (
                        columns_dot(present[:, at : at + HD], keys) * HD ** (-0.5) - slope * far
                    )
                    weight = jnp.where(allowed, jnp.exp(score), 0.0)
                    floor = jnp.exp(jnp.full((rows, 1), sink[local], F32))
                    probs = (weight / (jnp.sum(weight, axis=1, keepdims=True) + floor)).astype(BF)
                    results.append(dot(probs, vals))
                wide_to = heads * HD
                held_n[b, e, :, g * wide_to : (g + 1) * wide_to] = jnp.concatenate(
                    results, axis=1
                ).astype(BF)
            gather(e, b, 1).start()

        def collect(b):
            for i in range(2):
                gather(1 - e, b, i).wait_recv()

        states = [start[i].T for i in range(mine)]
        for b in range(sp):
            states = linear(b, states)
            window(b)
            if b == 1:
                loads[6].wait()
                loads[7].wait()
            if b:
                if b > 1:
                    close(b - 2)
                collect(b - 1)
                multiply(b - 1)
        close(sp - 2)
        collect(last)
        multiply(last)
        close(last)

    def drain(b, carry):
        for i in range(mine + 1):
            for way in range(2):

                @pl.when(s != last * (1 - way))
                def _():
                    step(way, b, i).wait_send()

        for i in range(2):
            for way in range(2):

                @pl.when(s != last * (1 - way))
                def _():
                    gather(way, b, i).wait_send()

        @pl.when(home)
        def _():
            forward(b).wait_send()

        return carry

    lax.fori_loop(0, sp, drain, 0)
    for i in range(per_half):

        @pl.when(t * per_half + i != s)
        def _():
            slice_send(i).wait_send()

    for n in range(2 * tp):
        send, away_from_here = note_send(n)

        @pl.when(away_from_here)
        def _():
            send.wait_send()

    columns = landed.shape[2]

    def leave(b):
        return pltpu.make_async_copy(
            landed.at[b], out.at[:, pl.ds(b * columns, columns)], y_sem.at[b]
        )

    for b in range(sp):

        @pl.when(s != b)
        def _():
            deliver(b).wait_send()
            remote(landed.at[b], landed.at[b], o_send.at[b], o_recv.at[b], tp=other).wait_recv()

        leave(b).start()
    for b in range(sp):
        leave(b).wait()


def stationary(
    activations,
    input_norm_gain,
    window_query_weight,
    window_key_weight,
    window_value_weight,
    linear_query_weight,
    linear_key_weight,
    linear_value_weight,
    decay_down_factor,
    decay_up_factor,
    decay_offset_bias,
    extra_fading_exponent,
    starting_state,
    head_sink_logit,
    linear_head_gain,
    window_output_weight,
    linear_output_weight,
):
    sp, tp = lax.axis_size("sp"), lax.axis_size("tp")
    rows, half = activations.shape
    matrices = (
        window_query_weight,
        window_key_weight,
        window_value_weight,
        linear_query_weight,
        linear_key_weight,
        linear_value_weight,
        window_output_weight,
        linear_output_weight,
    )
    rank = decay_down_factor.shape[1]
    heads_tp = extra_fading_exponent.shape[1]
    mine = heads_tp // 2
    noted = rank + heads_tp + -(rank + heads_tp) % 8
    columns = window_output_weight.shape[1]
    vmem = pl.BlockSpec(memory_space=pltpu.VMEM)
    hbm = pl.BlockSpec(memory_space=pltpu.HBM)
    dma = pltpu.SemaphoreType.DMA
    slice_width = half * tp // sp
    lin_cols = sum(m.shape[1] for m in matrices[3:6]) // heads_tp
    win_cols = sum(m.shape[1] for m in matrices[:3]) // 2
    return pl.pallas_call(
        functools.partial(mixer_kernel, sp, tp),
        out_shape=jax.ShapeDtypeStruct((rows // tp, columns * sp), BF),
        in_specs=[vmem] * 3
        + [pl.BlockSpec(memory_space=pltpu.SMEM)]
        + [vmem] * 3
        + [hbm] * 10,
        out_specs=hbm,
        scratch_shapes=[pltpu.VMEM(m.shape, BF) for m in matrices]
        + [
            pltpu.VMEM((mine,) + starting_state.shape[1:], F32),
            pltpu.VMEM((half, rank), BF),
            pltpu.VMEM((2, rows, 128), F32),
            pltpu.VMEM((sp // tp, rows, slice_width), BF),
            pltpu.VMEM((sp, rows, slice_width), BF),
            pltpu.VMEM((sp, tp, noted, rows), F32),
            pltpu.VMEM((sp, tp, rows // tp, columns), BF),
            pltpu.VMEM((sp, rows // tp, columns), BF),
            pltpu.VMEM((sp, rows // tp, columns), BF),
            pltpu.VMEM((sp, 2, mine, rows, lin_cols), BF),
            pltpu.VMEM((sp, 2, rows, win_cols), BF),
            pltpu.VMEM((2, sp, mine, rows, lin_cols), BF),
            pltpu.VMEM((2, sp, rows, win_cols), BF),
            pltpu.VMEM((sp, 2, rows, linear_output_weight.shape[0] // 2), BF),
            pltpu.VMEM((sp, 2, rows, window_output_weight.shape[0] // 2), BF),
            dma((10,)),
            dma((2,)),
            dma((sp // tp,)),
            dma((sp,)),
            dma((sp,)),
            dma,
            dma((2 * tp,)),
            dma((sp, tp)),
        ]
        + [dma((2, sp, mine + 1))] * 2
        + [dma((2, sp, 2))] * 2
        + [dma((sp,))] * 5,
        compiler_params=pltpu.CompilerParams(
            collective_id=0, has_side_effects=True, vmem_limit_bytes=56 * 2**20
        ),
    )(
        activations,
        input_norm_gain.reshape(tp, 1, half),
        decay_offset_bias.reshape(1, -1),
        head_sink_logit,
        linear_head_gain.reshape(1, -1),
        decay_up_factor,
        extra_fading_exponent,
        *matrices,
        starting_state,
        decay_down_factor,
    )


def mixer(*arrays):
    sp, tp = lax.axis_size("sp"), lax.axis_size("tp")
    rows = arrays[0].shape[0]
    one_each = KVH == GATED_MIXERS == sp * tp and QH % KVH == 0
    if tp == 2 and sp % tp == 0 and sp > 2 and one_each and rows == WINDOW and rows % SPAN == 0:
        return stationary(*arrays)
    return local(*arrays)


def solution(mesh):
    placed = (
        P(("fs", "sp"), "tp"),
        P(),
        P("sp", "tp"),
        P("sp", "tp"),
        P("sp", "tp"),
        P("sp", "tp"),
        P("sp", "tp"),
        P("sp", "tp"),
        P(),
        P(None, "tp"),
        P("tp"),
        P(("fs", "sp"), "tp"),
        P("tp", None, None),
        P("tp"),
        P(),
        P("tp", "sp"),
        P("tp", "sp"),
    )
    return jax.shard_map(
        mixer, mesh=mesh, in_specs=placed, out_specs=P(("fs", "sp", "tp"), None), check_vma=False
    )
```

time: 153 us -> 198 us (1.29)
  Pallas kernels: 149 us -> 192 us
    pallas_call x1, Pallas kernels: 149 us -> 192 us  [stationary(): pl.pallas_call(functools.partial(mixer_kernel, sp, tp), out_shape=jax.Sha...]
    unnamed x1 -> x3, local copies, waits for them, and re-layouts: 1.87 us -> 5.52 us
where the time goes in v1:
time: 198 us; the launch traced here: 197 us
  Pallas kernels  192 us (97%)
  local copies, waits for them, and re-layouts  5.52 us (3%)
    pallas_call x1, Pallas kernels, stationary(): pl.pallas_call(functools.partial(mixer_kernel, sp, tp), out_shape=jax.Sha...  192 us
    unnamed x3, local copies, waits for them, and re-layouts  5.52 us

profile of v1, /device:TPU:0, one launch (start us, length us, event | category | flops | bytes accessed | tf_op | source)
XLA Modules:
  0.0 197.2 jit_solution(2040931113884478900)
XLA Ops:
  0.0 1.4 copy.18.refs_6_
  1.4 2.2 %copy.19.refs_16_ = bf16[4096,16]{1,0:T(8,128)(2,1)} copy(bf16[4096,16]{0,1:T(8,128)(2,1)} %param.25) | data formatting | bytes 262144 | tf_op args[8]
  3.7 191.7 %shard_map.163 = bf16[64,4096]{1,0:T(8,128)(2,1)} custom-call(bf16[128,2048]{1,0:T(8,128)(2,1)} %refs_0_.1, f32[2,1,2048]{2,1,0:T(1,128)} %bitcast.3, f32[1,512]{1,0:T(1,128)} %bitcast.4, f32[16]{0:T(128)} %refs_3_.1, f32[1,256]{1,0:T(1,128)} %bitcast.5, bf16[16,512]{1,0:T(8,128)(2,1)} %refs_5_.1, f32[128,4]{1,0:T(8,128)} %copy.18.refs_6_, ...), custom_call_target="tpu_custom_call" | custom-call | tf_op jit(solution)/shard_map/pallas_call | solution.py:727
  195.3 1.9 copy.21

commit v2 on v1

--- a/solution.py
+++ b/solution.py
@@ -237,6 +237,7 @@
 MESH = pl.DeviceIdType.MESH
 BF = jnp.bfloat16
 F32 = jnp.float32
+LAG = 2
 
 
 def dot(a, b):
@@ -262,7 +263,10 @@
             if ds or dt:
                 where = {"sp": lax.rem(s + ds, sp), "tp": lax.rem(t + dt, tp)}
                 pl.semaphore_signal(barrier, inc=1, device_id=where, device_id_type=MESH)
-    pl.semaphore_wait(barrier, sp * tp - 1)
+
+
+def greeted(sp, tp):
+    pl.semaphore_wait(pltpu.get_barrier_semaphore(), sp * tp - 1)
 
 
 def columns_dot(a, b):
@@ -273,9 +277,9 @@
     x, gain, bias, sink, head_gain, up, fade = refs[:7]
     sources, state_in, down_in, out = refs[7:15], refs[15], refs[16], refs[17]
     weights, start, down = refs[18:26], refs[26], refs[27]
-    squares, normed, blocks, note, term, away, landed = refs[28:35]
-    lin_own, win_own, lin_in, win_in, held_g, held_n = refs[35:41]
-    w_sem, sq_sem, a_send, a_recv, f_send, l_sem, n_send, n_recv = refs[41:49]
+    squares, blocks, note, term, away, landed = refs[28:34]
+    lin_own, win_own, lin_in, win_in, held_g, held_n = refs[34:40]
+    w_sem, sq_send, sq_recv, a_send, a_recv, f_send, l_sem, n_send, n_recv = refs[40:49]
     r_send, r_recv, g_send, g_recv, t_send, t_recv, o_send, o_recv, y_sem = refs[49:58]
     s, t = lax.axis_index("sp"), lax.axis_index("tp")
     other = 1 - t
@@ -290,6 +294,7 @@
     lk = LOOKUP_FEATURES
     mine = lin_own.shape[2]
     lane_of = {i: weights[i].shape[1] // 2 for i in range(6)}
+    greet(sp, tp)
     loads = [
         pltpu.make_async_copy(a, b, w_sem.at[i]) for i, (a, b) in enumerate(zip(sources, weights))
     ]
@@ -303,44 +308,59 @@
         loads[i].start()
     wide = x[...].astype(F32)
     own = jnp.sum(wide * wide, axis=1, keepdims=True)
-    squares[0] = jnp.broadcast_to(own, (rows, 128))
-    greet(sp, tp)
-    swap_squares = remote(squares.at[0], squares.at[1], sq_sem.at[0], sq_sem.at[1], tp=other)
-    swap_squares.start()
-    swap_squares.wait()
-    total = own + squares[1][:, :1]
-    scale = lax.rsqrt(total / (half * tp) + EPS)
+    squares[s, t] = jnp.broadcast_to(own, (rows, rows)).T[:8]
     home = lax.div(s, per_half) == t
 
     def slice_send(i):
-        j = t * per_half + i
-        return remote(normed.at[i], blocks.at[s], a_send.at[i], a_recv.at[s], sp=j)
-
-    for i in range(per_half):
-        cols = slice(i * width, (i + 1) * width)
-        normed[i] = (x[:, cols].astype(F32) * scale * gain[t, :, cols]).astype(BF)
-
-        @pl.when(t * per_half + i != s)
-        def _():
-            slice_send(i).start()
-
-        @pl.when(t * per_half + i == s)
-        def _():
-            keep = pltpu.make_async_copy(normed.at[i], blocks.at[s], l_sem)
-            keep.start()
-            keep.wait()
+        src = x.at[:, i * width : (i + 1) * width]
+        return remote(src, blocks.at[s], a_send.at[i], a_recv.at[s], sp=t * per_half + i)
 
     def forward(b):
         return remote(blocks.at[b], blocks.at[b], f_send.at[b], a_recv.at[b], tp=other)
 
-    @pl.when(home)
-    def _():
-        forward(s).start()
-
+    def squares_send(n):
+        where = {"sp": lax.rem(s + n // tp, sp), "tp": lax.rem(t + n % tp, tp)}
+        ref = squares.at[s, t]
+        return remote(ref, ref, sq_send.at[n], sq_recv.at[s, t], **where)
+
+    def keep(i):
+        return pltpu.make_async_copy(x.at[:, i * width : (i + 1) * width], blocks.at[s], l_sem)
+
+    def share(i):
+        src = x.at[:, i * width : (i + 1) * width]
+        return remote(src, blocks.at[s], f_send.at[s], a_recv.at[s], tp=other)
+
+    greeted(sp, tp)
+    for n in range(1, sp * tp):
+        squares_send(n).start()
+    for i in range(per_half):
+
+        @pl.when(t * per_half + i != s)
+        def _():
+            slice_send(i).start()
+
+        @pl.when(t * per_half + i == s)
+        def _():
+            share(i).start()
+            keep(i).start()
+
+    def squares_wait(ps, pt):
+        ref = squares.at[ps, pt]
+        remote(ref, ref, sq_send.at[0], sq_recv.at[ps, pt], tp=other).wait_recv()
+
+    def scale_of(b):
+        total = jnp.sum(squares[b], axis=0) / (half * tp)
+        tall = jnp.concatenate([lax.rsqrt(total + EPS), jnp.zeros((rows - 8, rows), F32)], axis=0)
+        return tall.T[:, :1]
+
+    squares_wait(s, other)
+    scale = scale_of(s)
     loads[9].wait()
     low = jnp.zeros((rows, rank), F32)
     for i in range(per_half):
-        low += dot(normed[i], down[i * width : (i + 1) * width])
+        cols = slice(i * width, (i + 1) * width)
+        shaped = (x[:, cols].astype(F32) * scale * gain[t, :, cols]).astype(BF)
+        low += dot(shaped, down[cols])
     fades = fade.shape[1]
     noted = note.shape[2]
     wide_note = jnp.concatenate(
@@ -369,22 +389,22 @@
             src, dst, r_send.at[way, b, i], r_recv.at[way, b, i], sp=jnp.clip(s + 1 - 2 * way, 0, last)
         )
 
-    def relay(way, b):
-        for i in range(mine + 1):
-            step(way, b, i).wait_recv()
-            if i < mine:
-                lin_own[b, 1 - way, i] = (
-                    lin_own[b, 1 - way, i].astype(F32) + lin_in[way, b, i].astype(F32)
-                ).astype(BF)
-            else:
-                win_own[b, 1 - way] = (
-                    win_own[b, 1 - way].astype(F32) + win_in[way, b].astype(F32)
-                ).astype(BF)
-            step(way, b, i).start()
+    def relay(way, b, i):
+        step(way, b, i).wait_recv()
+        if i < mine:
+            lin_own[b, 1 - way, i] = (
+                lin_own[b, 1 - way, i].astype(F32) + lin_in[way, b, i].astype(F32)
+            ).astype(BF)
+        else:
+            win_own[b, 1 - way] = (
+                win_own[b, 1 - way].astype(F32) + win_in[way, b].astype(F32)
+            ).astype(BF)
+        step(way, b, i).start()
 
     for i in range(6):
         loads[i].wait()
     qw, kw = lane_of[0], lane_of[1]
+    gain_here = gain[lax.div(s, per_half), :, pl.ds(pl.multiple_of(lax.rem(s, per_half) * width, width), width)]
 
     def project(b, carry):
         @pl.when(jnp.logical_or(jnp.logical_not(home), b != s))
@@ -395,7 +415,16 @@
         def _():
             forward(b).start()
 
-        block = blocks[b]
+        @pl.when(jnp.logical_and(home, b == s))
+        def _():
+            keep(0).wait()
+
+        @pl.when(b != s)
+        def _():
+            for pt in range(tp):
+                squares_wait(b, pt)
+
+        block = (blocks[b].astype(F32) * scale_of(b) * gain_here).astype(BF)
 
         def part(i, h):
             w = lane_of[i]
@@ -423,14 +452,6 @@
                 @pl.when(at_end)
                 def _():
                     step(e, b, mine).start()
-
-        @pl.when(jnp.logical_and(inside, b >= 1))
-        def _():
-            relay(0, b - 1)
-
-        @pl.when(jnp.logical_and(inside, b >= 2))
-        def _():
-            relay(1, b - 2)
 
         return carry
 
@@ -474,28 +495,32 @@
             term[b, h] = total[h * part_rows : (h + 1) * part_rows].astype(BF)
         swap(b).start()
 
-    def pass_on(b):
-        for i in range(2):
-            for way in range(2):
-                gather(way, b, i).wait_recv()
-                gather(way, b, i).start()
+    def pass_on(way, b, i):
+        gather(way, b, i).wait_recv()
+        gather(way, b, i).start()
 
     @pl.when(inside)
     def _():
         loads[8].wait()
-        relay(1, sp - 2)
-        pass_on(0)
-        relay(0, last)
-        relay(1, last)
-        pass_on(1)
+        sums = [(b, i) for b in range(sp) for i in range(mine + 1)]
+        for n in range(len(sums) + LAG):
+            if n < len(sums):
+                relay(e, *sums[n])
+            if n >= LAG:
+                relay(1 - e, *sums[n - LAG])
         loads[6].wait()
         loads[7].wait()
-        for b in range(sp):
-            multiply(b)
-            if b + 2 < sp:
-                pass_on(b + 2)
-            if b:
-                close(b - 1)
+        outs = [(b, i) for b in range(sp) for i in range(2)]
+        for n in range(len(outs) + LAG):
+            if n < len(outs):
+                pass_on(e, *outs[n])
+            if n >= LAG:
+                b, i = outs[n - LAG]
+                pass_on(1 - e, b, i)
+                if i == 1:
+                    multiply(b)
+                    if b:
+                        close(b - 1)
         close(last)
 
     @pl.when(at_end)
@@ -615,17 +640,13 @@
         for b in range(sp):
             states = linear(b, states)
             window(b)
-            if b == 1:
-                loads[6].wait()
-                loads[7].wait()
+        loads[6].wait()
+        loads[7].wait()
+        for b in range(sp):
+            collect(b)
+            multiply(b)
             if b:
-                if b > 1:
-                    close(b - 2)
-                collect(b - 1)
-                multiply(b - 1)
-        close(sp - 2)
-        collect(last)
-        multiply(last)
+                close(b - 1)
         close(last)
 
     def drain(b, carry):
@@ -662,6 +683,9 @@
         @pl.when(away_from_here)
         def _():
             send.wait_send()
+
+    for n in range(1, sp * tp):
+        squares_send(n).wait_send()
 
     columns = landed.shape[2]
 
@@ -736,8 +760,7 @@
         + [
             pltpu.VMEM((mine,) + starting_state.shape[1:], F32),
             pltpu.VMEM((half, rank), BF),
-            pltpu.VMEM((2, rows, 128), F32),
-            pltpu.VMEM((sp // tp, rows, slice_width), BF),
+            pltpu.VMEM((sp, tp, 8, rows), F32),
             pltpu.VMEM((sp, rows, slice_width), BF),
             pltpu.VMEM((sp, tp, noted, rows), F32),
             pltpu.VMEM((sp, tp, rows // tp, columns), BF),
@@ -750,7 +773,8 @@
             pltpu.VMEM((sp, 2, rows, linear_output_weight.shape[0] // 2), BF),
             pltpu.VMEM((sp, 2, rows, window_output_weight.shape[0] // 2), BF),
             dma((10,)),
-            dma((2,)),
+            dma((sp * tp,)),
+            dma((sp, tp)),
             dma((sp // tp,)),
             dma((sp,)),
             dma((sp,)),

time: 198 us -> 119 us (0.60)
  Pallas kernels: 192 us -> 113 us
    pallas_call x1, Pallas kernels: 192 us -> 113 us  [stationary(): pl.pallas_call(functools.partial(mixer_kernel, sp, tp), out_shape=jax.Sha...]
where the time goes in v2:
time: 119 us; the launch traced here: 118 us
  Pallas kernels  113 us (95%)
  local copies, waits for them, and re-layouts  5.52 us (5%)
    pallas_call x1, Pallas kernels, stationary(): pl.pallas_call(functools.partial(mixer_kernel, sp, tp), out_shape=jax.Sha...  113 us
    unnamed x3, local copies, waits for them, and re-layouts  5.52 us

profile of v2, /device:TPU:0, one launch (start us, length us, event | category | flops | bytes accessed | tf_op | source)
XLA Modules:
  0.0 118.2 jit_solution(11991913189934731618)
XLA Ops:
  0.0 1.4 %copy.18.refs_6_ = f32[128,4]{1,0:T(8,128)} copy(f32[128,4]{0,1:T(4,128)} %param.28) | data formatting | bytes 4096 | tf_op args[11]
  1.4 2.2 %copy.19.refs_16_ = bf16[4096,16]{1,0:T(8,128)(2,1)} copy(bf16[4096,16]{0,1:T(8,128)(2,1)} %param.25) | data formatting | bytes 262144 | tf_op args[8]
  3.7 112.7 %shard_map.163 = bf16[64,4096]{1,0:T(8,128)(2,1)} custom-call(bf16[128,2048]{1,0:T(8,128)(2,1)} %refs_0_.1, f32[2,1,2048]{2,1,0:T(1,128)} %bitcast.3, f32[1,512]{1,0:T(1,128)} %bitcast.4, f32[16]{0:T(128)} %refs_3_.1, f32[1,256]{1,0:T(1,128)} %bitcast.5, bf16[16,512]{1,0:T(8,128)(2,1)} %refs_5_.1, f32[128,4]{1,0:T(8,128)} %copy.18.refs_6_, ...), custom_call_target="tpu_custom_call" | custom-call | tf_op jit(solution)/shard_map/pallas_call | solution.py:751
  116.3 1.9 %copy.21 = bf16[64,4096]{1,0:T(8,128)(2,1)} copy(bf16[64,4096]{1,0:T(8,128)(2,1)} %shard_map.163) | data formatting | bytes 1048576

commit v3 on v2

--- a/solution.py
+++ b/solution.py
@@ -238,6 +238,7 @@
 BF = jnp.bfloat16
 F32 = jnp.float32
 LAG = 2
+CUTS = 2
 
 
 def dot(a, b):
@@ -274,13 +275,13 @@
 
 
 def mixer_kernel(sp, tp, *refs):
-    x, gain, bias, sink, head_gain, up, fade = refs[:7]
-    sources, state_in, down_in, out = refs[7:15], refs[15], refs[16], refs[17]
-    weights, start, down = refs[18:26], refs[26], refs[27]
-    squares, blocks, note, term, away, landed = refs[28:34]
-    lin_own, win_own, lin_in, win_in, held_g, held_n = refs[34:40]
-    w_sem, sq_send, sq_recv, a_send, a_recv, f_send, l_sem, n_send, n_recv = refs[40:49]
-    r_send, r_recv, g_send, g_recv, t_send, t_recv, o_send, o_recv, y_sem = refs[49:58]
+    gain, bias, sink, head_gain, up, fade = refs[:6]
+    sources, state_in, down_in, x_in, out = refs[6:14], refs[14], refs[15], refs[16], refs[17]
+    weights, start, down, x = refs[18:26], refs[26], refs[27], refs[28]
+    squares, blocks, note, term, away, landed = refs[29:35]
+    lin_own, win_own, lin_in, win_in, held_g, held_n = refs[35:41]
+    w_sem, sq_send, sq_recv, a_send, a_recv, f_send, l_sem, n_send, n_recv = refs[41:50]
+    r_send, r_recv, g_send, g_recv, t_send, t_recv, o_send, o_recv, y_sem, turn = refs[50:60]
     s, t = lax.axis_index("sp"), lax.axis_index("tp")
     other = 1 - t
     last = sp - 1
@@ -290,7 +291,7 @@
     per_half = sp // tp
     rows, half = x.shape
     width = half // per_half
-    rank = down.shape[1]
+    rank = down.shape[0]
     lk = LOOKUP_FEATURES
     mine = lin_own.shape[2]
     lane_of = {i: weights[i].shape[1] // 2 for i in range(6)}
@@ -301,11 +302,13 @@
     loads.append(pltpu.make_async_copy(state_in.at[pl.ds(e * mine, mine)], start, w_sem.at[8]))
     loads.append(
         pltpu.make_async_copy(
-            down_in.at[pl.ds(pl.multiple_of(t * half, half), half)], down, w_sem.at[9]
+            down_in.at[:, pl.ds(pl.multiple_of(t * half, half), half)], down, w_sem.at[9]
         )
     )
-    for i in (9, 3, 4, 5, 0, 1, 2, 8, 6, 7):
+    loads.append(pltpu.make_async_copy(x_in, x, w_sem.at[10]))
+    for i in (10, 9, 3, 4, 5, 0, 1, 2, 8, 6, 7):
         loads[i].start()
+    loads[10].wait()
     wide = x[...].astype(F32)
     own = jnp.sum(wide * wide, axis=1, keepdims=True)
     squares[s, t] = jnp.broadcast_to(own, (rows, rows)).T[:8]
@@ -333,13 +336,14 @@
     greeted(sp, tp)
     for n in range(1, sp * tp):
         squares_send(n).start()
-    for i in range(per_half):
-
-        @pl.when(t * per_half + i != s)
+    for i in reversed(range(per_half)):
+        j = t * per_half + i
+
+        @pl.when((j < s) | ((j > s) & (s == 0) & (t > 0)))
         def _():
             slice_send(i).start()
 
-        @pl.when(t * per_half + i == s)
+        @pl.when(j == s)
         def _():
             share(i).start()
             keep(i).start()
@@ -356,17 +360,16 @@
     squares_wait(s, other)
     scale = scale_of(s)
     loads[9].wait()
-    low = jnp.zeros((rows, rank), F32)
+    low = jnp.zeros((rank, rows), F32)
     for i in range(per_half):
         cols = slice(i * width, (i + 1) * width)
         shaped = (x[:, cols].astype(F32) * scale * gain[t, :, cols]).astype(BF)
-        low += dot(shaped, down[cols])
-    fades = fade.shape[1]
+        low += columns_dot(down[:, cols], shaped)
+    fades = fade.shape[0]
     noted = note.shape[2]
-    wide_note = jnp.concatenate(
-        [low, fade[...], jnp.zeros((rows, rows - rank - fades), F32)], axis=1
-    )
-    note[s, t] = wide_note.T[:noted]
+    note[s, t] = jnp.concatenate(
+        [low, fade[...], jnp.zeros((noted - rank - fades, rows), F32)], axis=0
+    )
 
     def note_send(n):
         place, core = (0 if n < tp else last), lax.rem(t + n % tp, tp)
@@ -382,31 +385,46 @@
         def _():
             send.start()
 
-    def step(way, b, i):
-        src = lin_own.at[b, 1 - way, i] if i < mine else win_own.at[b, 1 - way]
-        dst = lin_in.at[way, b, i] if i < mine else win_in.at[way, b]
+    cut_rows = rows // CUTS
+    pieces = [(i, slice(r * cut_rows, (r + 1) * cut_rows)) for i in range(mine + 1) for r in range(CUTS)]
+
+    def step(way, b, n):
+        i, cut = pieces[n]
+        src = lin_own.at[b, 1 - way, i, cut] if i < mine else win_own.at[b, 1 - way, cut]
+        dst = lin_in.at[way, b, i, cut] if i < mine else win_in.at[way, b, cut]
         return remote(
-            src, dst, r_send.at[way, b, i], r_recv.at[way, b, i], sp=jnp.clip(s + 1 - 2 * way, 0, last)
+            src, dst, r_send.at[way, b, n], r_recv.at[way, b, n], sp=jnp.clip(s + 1 - 2 * way, 0, last)
         )
 
-    def relay(way, b, i):
-        step(way, b, i).wait_recv()
+    def relay(way, b, n):
+        i, cut = pieces[n]
+        step(way, b, n).wait_recv()
         if i < mine:
-            lin_own[b, 1 - way, i] = (
-                lin_own[b, 1 - way, i].astype(F32) + lin_in[way, b, i].astype(F32)
+            lin_own[b, 1 - way, i, cut] = (
+                lin_own[b, 1 - way, i, cut].astype(F32) + lin_in[way, b, i, cut].astype(F32)
             ).astype(BF)
         else:
-            win_own[b, 1 - way] = (
-                win_own[b, 1 - way].astype(F32) + win_in[way, b].astype(F32)
+            win_own[b, 1 - way, cut] = (
+                win_own[b, 1 - way, cut].astype(F32) + win_in[way, b, cut].astype(F32)
             ).astype(BF)
-        step(way, b, i).start()
+        step(way, b, n).start()
 
     for i in range(6):
         loads[i].wait()
     qw, kw = lane_of[0], lane_of[1]
     gain_here = gain[lax.div(s, per_half), :, pl.ds(pl.multiple_of(lax.rem(s, per_half) * width, width), width)]
 
-    def project(b, carry):
+    def send_sums(b):
+        for n in range(len(pieces)):
+            step(e, b, n).start()
+
+    def project(k, carry):
+        b = lax.rem(s + k, sp)
+
+        @pl.when((s > 1) & inside & (k == sp - 1))
+        def _():
+            relay(e, 0, 0)
+
         @pl.when(jnp.logical_or(jnp.logical_not(home), b != s))
         def _():
             forward(b).wait_recv()
@@ -423,6 +441,12 @@
         def _():
             for pt in range(tp):
                 squares_wait(b, pt)
+
+        for i in reversed(range(per_half)):
+
+            @pl.when((b == 0) & (s > 1) & (t * per_half + i > s))
+            def _():
+                slice_send(i).start()
 
         block = (blocks[b].astype(F32) * scale_of(b) * gain_here).astype(BF)
 
@@ -439,28 +463,51 @@
                 lin_own[b, h, i, :, 2 * lk :] = value[:, i * DV : (i + 1) * DV]
             if n == 0:
 
-                @pl.when(at_end)
+                @pl.when((s == 0) & (t > 0) & (k == 0))
                 def _():
-                    for i in range(mine):
-                        step(e, b, i).start()
+                    slice_send(per_half - 1).wait_send()
+                    pl.semaphore_signal(turn, inc=1, device_id={"tp": other}, device_id_type=MESH)
+
+                @pl.when((s == 0) & (t == 0) & (k == 0))
+                def _():
+                    pl.semaphore_wait(turn, 1)
+                    for i in range(1, per_half):
+                        slice_send(i).start()
+
+                for i in reversed(range(per_half)):
+
+                    @pl.when((k == 0) & (s == 1) & (t * per_half + i > s))
+                    def _():
+                        slice_send(i).start()
+
+                @pl.when(at_end & (k >= e))
+                def _():
+                    for m in range(mine * CUTS):
+                        step(e, b, m).start()
 
             win_own[b, h, :, :qw] = part(0, h)
             win_own[b, h, :, qw : qw + kw] = part(1, h)
             win_own[b, h, :, qw + kw :] = part(2, h)
             if n == 0:
 
-                @pl.when(at_end)
+                @pl.when(at_end & (k >= e))
                 def _():
-                    step(e, b, mine).start()
+                    for m in range(mine * CUTS, len(pieces)):
+                        step(e, b, m).start()
 
         return carry
 
     lax.fori_loop(0, sp, project, 0)
 
-    def gather(way, b, i):
-        ref = (held_g if i == 0 else held_n).at[b, way]
+    @pl.when(s == last)
+    def _():
+        send_sums(last)
+
+    def gather(way, b, n):
+        i, r = divmod(n, CUTS)
+        ref = (held_n if i else held_g).at[b, way, slice(r * cut_rows, (r + 1) * cut_rows)]
         return remote(
-            ref, ref, g_send.at[way, b, i], g_recv.at[way, b, i], sp=jnp.clip(s + 1 - 2 * way, 0, last)
+            ref, ref, g_send.at[way, b, n], g_recv.at[way, b, n], sp=jnp.clip(s + 1 - 2 * way, 0, last)
         )
 
     part_rows = rows // tp
@@ -502,26 +549,31 @@
     @pl.when(inside)
     def _():
         loads[8].wait()
-        sums = [(b, i) for b in range(sp) for i in range(mine + 1)]
-        for n in range(len(sums) + LAG):
-            if n < len(sums):
-                relay(e, *sums[n])
+        items = [(relay, b, i) for b in range(sp) for i in range(len(pieces))]
+        items += [(pass_on, b, i) for b in range(sp) for i in range(2 * CUTS)]
+        for n in range(len(items) + LAG):
+            if n == 0:
+
+                @pl.when(s <= 1)
+                def _():
+                    relay(e, 0, 0)
+
+            elif n < len(items):
+                what, b, i = items[n]
+                what(e, b, i)
             if n >= LAG:
-                relay(1 - e, *sums[n - LAG])
-        loads[6].wait()
-        loads[7].wait()
-        outs = [(b, i) for b in range(sp) for i in range(2)]
-        for n in range(len(outs) + LAG):
-            if n < len(outs):
-                pass_on(e, *outs[n])
-            if n >= LAG:
-                b, i = outs[n - LAG]
-                pass_on(1 - e, b, i)
-                if i == 1:
+                what, b, i = items[n - LAG]
+                what(1 - e, b, i)
+                if what is pass_on and i == 2 * CUTS - 1:
+                    if b == 0:
+                        loads[6].wait()
+                        loads[7].wait()
+                    if b == last:
+                        for c in range(1, last):
+                            close(c)
                     multiply(b)
-                    if b:
-                        close(b - 1)
         close(last)
+        close(0)
 
     @pl.when(at_end)
     def _():
@@ -572,7 +624,8 @@
             running_all = summed[:, :span] + (summed[:, span : 2 * span] + summed[:, 2 * span :])
             new_states = []
             for i in range(mine):
-                step(1 - e, b, i).wait_recv()
+                for r in range(CUTS):
+                    step(1 - e, b, i * CUTS + r).wait_recv()
                 here = (lin_own[b, e, i].astype(F32) + lin_in[1 - e, b, i].astype(F32)).astype(BF)
                 running = running_all[:, i * lk : (i + 1) * lk]
                 state = states[i]
@@ -600,11 +653,13 @@
                 )
                 held_g[b, e, :, i * DV : (i + 1) * DV] = normal.astype(BF)
                 new_states.append(state)
-            gather(e, b, 0).start()
+            for r in range(CUTS):
+                gather(e, b, r).start()
             return new_states
 
         def window(b):
-            step(1 - e, b, mine).wait_recv()
+            for r in range(CUTS):
+                step(1 - e, b, mine * CUTS + r).wait_recv()
             win_own[b, e] = (win_own[b, e].astype(F32) + win_in[1 - e, b].astype(F32)).astype(BF)
             present = win_own[b, e]
             earlier = win_own[max(b - 1, 0), e]
@@ -630,10 +685,11 @@
                 held_n[b, e, :, g * wide_to : (g + 1) * wide_to] = jnp.concatenate(
                     results, axis=1
                 ).astype(BF)
-            gather(e, b, 1).start()
+            for r in range(CUTS):
+                gather(e, b, CUTS + r).start()
 
         def collect(b):
-            for i in range(2):
+            for i in range(2 * CUTS):
                 gather(1 - e, b, i).wait_recv()
 
         states = [start[i].T for i in range(mine)]
@@ -645,19 +701,20 @@
         for b in range(sp):
             collect(b)
             multiply(b)
-            if b:
-                close(b - 1)
+            if b == last - 1:
+                for c in (*range(1, last), 0):
+                    close(c)
         close(last)
 
     def drain(b, carry):
-        for i in range(mine + 1):
+        for i in range(len(pieces)):
             for way in range(2):
 
                 @pl.when(s != last * (1 - way))
                 def _():
                     step(way, b, i).wait_send()
 
-        for i in range(2):
+        for i in range(2 * CUTS):
             for way in range(2):
 
                 @pl.when(s != last * (1 - way))
@@ -673,7 +730,7 @@
     lax.fori_loop(0, sp, drain, 0)
     for i in range(per_half):
 
-        @pl.when(t * per_half + i != s)
+        @pl.when((t * per_half + i != s) & ((s > 0) | (t == 0) | (i < per_half - 1)))
         def _():
             slice_send(i).wait_send()
 
@@ -751,15 +808,16 @@
     return pl.pallas_call(
         functools.partial(mixer_kernel, sp, tp),
         out_shape=jax.ShapeDtypeStruct((rows // tp, columns * sp), BF),
-        in_specs=[vmem] * 3
+        in_specs=[vmem] * 2
         + [pl.BlockSpec(memory_space=pltpu.SMEM)]
         + [vmem] * 3
-        + [hbm] * 10,
+        + [hbm] * 11,
         out_specs=hbm,
         scratch_shapes=[pltpu.VMEM(m.shape, BF) for m in matrices]
         + [
             pltpu.VMEM((mine,) + starting_state.shape[1:], F32),
-            pltpu.VMEM((half, rank), BF),
+            pltpu.VMEM((rank, half), BF),
+            pltpu.VMEM((rows, half), BF),
             pltpu.VMEM((sp, tp, 8, rows), F32),
             pltpu.VMEM((sp, rows, slice_width), BF),
             pltpu.VMEM((sp, tp, noted, rows), F32),
@@ -772,7 +830,7 @@
             pltpu.VMEM((2, sp, rows, win_cols), BF),
             pltpu.VMEM((sp, 2, rows, linear_output_weight.shape[0] // 2), BF),
             pltpu.VMEM((sp, 2, rows, window_output_weight.shape[0] // 2), BF),
-            dma((10,)),
+            dma((11,)),
             dma((sp * tp,)),
             dma((sp, tp)),
             dma((sp // tp,)),
@@ -782,23 +840,24 @@
             dma((2 * tp,)),
             dma((sp, tp)),
         ]
-        + [dma((2, sp, mine + 1))] * 2
-        + [dma((2, sp, 2))] * 2
-        + [dma((sp,))] * 5,
+        + [dma((2, sp, (mine + 1) * CUTS))] * 2
+        + [dma((2, sp, 2 * CUTS))] * 2
+        + [dma((sp,))] * 5
+        + [pltpu.SemaphoreType.REGULAR],
         compiler_params=pltpu.CompilerParams(
             collective_id=0, has_side_effects=True, vmem_limit_bytes=56 * 2**20
         ),
     )(
-        activations,
         input_norm_gain.reshape(tp, 1, half),
         decay_offset_bias.reshape(1, -1),
         head_sink_logit,
         linear_head_gain.reshape(1, -1),
         decay_up_factor,
-        extra_fading_exponent,
+        extra_fading_exponent.T,
         *matrices,
         starting_state,
-        decay_down_factor,
+        decay_down_factor.T,
+        activations,
     )
 
 

time: 119 us -> 104 us (0.87)
  Pallas kernels: 113 us -> 101 us
  local copies, waits for them, and re-layouts: 5.52 us -> 1.87 us
    pallas_call x1, Pallas kernels: 113 us -> 101 us  [stationary(): pl.pallas_call(functools.partial(mixer_kernel, sp, tp), out_shape=jax.Sha...]
    unnamed x3 -> x1, local copies, waits for them, and re-layouts: 5.52 us -> 1.87 us
where the time goes in v3:
time: 104 us; the launch traced here: 103 us
  Pallas kernels  101 us (97%)
  local copies, waits for them, and re-layouts  1.87 us (2%)
    pallas_call x1, Pallas kernels, stationary(): pl.pallas_call(functools.partial(mixer_kernel, sp, tp), out_shape=jax.Sha...  101 us

profile of v3, /device:TPU:0, one launch (start us, length us, event | category | flops | bytes accessed | tf_op | source)
XLA Modules:
  0.0 103.3 jit_solution(309068897636142197)
XLA Ops:
  0.0 101.4 %shard_map.163 = bf16[64,4096]{1,0:T(8,128)(2,1)} custom-call(f32[2,1,2048]{2,1,0:T(1,128)} %bitcast.6, f32[1,512]{1,0:T(1,128)} %bitcast.7, f32[16]{0:T(128)} %refs_2_.1, f32[1,256]{1,0:T(1,128)} %bitcast.9, bf16[16,512]{1,0:T(8,128)(2,1)} %refs_4_.1, f32[4,128]{1,0:T(4,128)} %bitcast.8, bf16[1024,1024]{1,0:T(8,128)(2,1)} %refs_6_.1, ...), custom_call_target="tpu_custom_call" | custom-call | tf_op jit(solution)/shard_map/pallas_call | solution.py:808
  101.4 1.9 %copy.19 = bf16[64,4096]{1,0:T(8,128)(2,1)} copy(bf16[64,4096]{1,0:T(8,128)(2,1)} %shard_map.163) | data formatting | bytes 1048576

commit v4 on v3

--- a/solution.py
+++ b/solution.py
@@ -239,6 +239,7 @@
 F32 = jnp.float32
 LAG = 2
 CUTS = 2
+EARLY = 3
 
 
 def dot(a, b):
@@ -275,13 +276,14 @@
 
 
 def mixer_kernel(sp, tp, *refs):
-    gain, bias, sink, head_gain, up, fade = refs[:6]
-    sources, state_in, down_in, x_in, out = refs[6:14], refs[14], refs[15], refs[16], refs[17]
+    small_in, sources, state_in, down_in, x_in = refs[:6], refs[6:14], refs[14], refs[15], refs[16]
+    out = refs[17]
     weights, start, down, x = refs[18:26], refs[26], refs[27], refs[28]
-    squares, blocks, note, term, away, landed = refs[29:35]
-    lin_own, win_own, lin_in, win_in, held_g, held_n = refs[35:41]
-    w_sem, sq_send, sq_recv, a_send, a_recv, f_send, l_sem, n_send, n_recv = refs[41:50]
-    r_send, r_recv, g_send, g_recv, t_send, t_recv, o_send, o_recv, y_sem, turn = refs[50:60]
+    gain, bias, sink, head_gain, up, fade = refs[59:65]
+    squares, blocks, note, term, away = refs[29:34]
+    lin_own, win_own, lin_in, win_in, held_g, held_n = refs[34:40]
+    w_sem, sq_send, sq_recv, a_send, a_recv, f_send, l_sem, n_send, n_recv = refs[40:49]
+    r_send, r_recv, g_send, g_recv, t_send, t_recv, o_send, o_recv, turn, s_sem = refs[49:59]
     s, t = lax.axis_index("sp"), lax.axis_index("tp")
     other = 1 - t
     last = sp - 1
@@ -306,33 +308,41 @@
         )
     )
     loads.append(pltpu.make_async_copy(x_in, x, w_sem.at[10]))
-    for i in (10, 9, 3, 4, 5, 0, 1, 2, 8, 6, 7):
+    small = [
+        pltpu.make_async_copy(a, b, s_sem.at[i]) for i, (a, b) in enumerate(zip(small_in, refs[59:65]))
+    ]
+    loads[10].start()
+    for copy in small:
+        copy.start()
+    for i in (9, 3, 4, 5, 0, 1, 2, 8, 6, 7):
         loads[i].start()
+    home = lax.div(s, per_half) == t
+
+    def slice_send(i):
+        src = x.at[:, i * width : (i + 1) * width]
+        return remote(src, blocks.at[s], a_send.at[i], a_recv.at[s], sp=t * per_half + i)
+
+    def forward(b):
+        return remote(blocks.at[b], blocks.at[b], f_send, a_recv.at[b], tp=other)
+
+    me = s * tp + t
+
+    def squares_send(n):
+        where = {"sp": lax.rem(s + n // tp, sp), "tp": lax.rem(t + n % tp, tp)}
+        ref = squares.at[me]
+        return remote(ref, ref, sq_send, sq_recv.at[0 if n // tp == 0 else 1], **where)
+
+    def keep(i):
+        return pltpu.make_async_copy(x.at[:, i * width : (i + 1) * width], blocks.at[s], l_sem)
+
+    def share(i):
+        src = x.at[:, i * width : (i + 1) * width]
+        return remote(src, blocks.at[s], f_send, a_recv.at[s], tp=other)
+
     loads[10].wait()
     wide = x[...].astype(F32)
     own = jnp.sum(wide * wide, axis=1, keepdims=True)
-    squares[s, t] = jnp.broadcast_to(own, (rows, rows)).T[:8]
-    home = lax.div(s, per_half) == t
-
-    def slice_send(i):
-        src = x.at[:, i * width : (i + 1) * width]
-        return remote(src, blocks.at[s], a_send.at[i], a_recv.at[s], sp=t * per_half + i)
-
-    def forward(b):
-        return remote(blocks.at[b], blocks.at[b], f_send.at[b], a_recv.at[b], tp=other)
-
-    def squares_send(n):
-        where = {"sp": lax.rem(s + n // tp, sp), "tp": lax.rem(t + n % tp, tp)}
-        ref = squares.at[s, t]
-        return remote(ref, ref, sq_send.at[n], sq_recv.at[s, t], **where)
-
-    def keep(i):
-        return pltpu.make_async_copy(x.at[:, i * width : (i + 1) * width], blocks.at[s], l_sem)
-
-    def share(i):
-        src = x.at[:, i * width : (i + 1) * width]
-        return remote(src, blocks.at[s], f_send.at[s], a_recv.at[s], tp=other)
-
+    squares[me] = jnp.broadcast_to(own, (rows, rows)).T[:8]
     greeted(sp, tp)
     for n in range(1, sp * tp):
         squares_send(n).start()
@@ -348,16 +358,18 @@
             share(i).start()
             keep(i).start()
 
-    def squares_wait(ps, pt):
-        ref = squares.at[ps, pt]
-        remote(ref, ref, sq_send.at[0], sq_recv.at[ps, pt], tp=other).wait_recv()
+    def squares_wait(n, k):
+        ref = squares.at[pl.ds(0, n)]
+        remote(ref, ref, sq_send, sq_recv.at[k], tp=other).wait_recv()
 
     def scale_of(b):
-        total = jnp.sum(squares[b], axis=0) / (half * tp)
+        total = (squares[b * tp] + squares[b * tp + 1]) / (half * tp)
         tall = jnp.concatenate([lax.rsqrt(total + EPS), jnp.zeros((rows - 8, rows), F32)], axis=0)
         return tall.T[:, :1]
 
-    squares_wait(s, other)
+    for copy in small:
+        copy.wait()
+    squares_wait(tp - 1, 0)
     scale = scale_of(s)
     loads[9].wait()
     low = jnp.zeros((rank, rows), F32)
@@ -366,17 +378,15 @@
         shaped = (x[:, cols].astype(F32) * scale * gain[t, :, cols]).astype(BF)
         low += columns_dot(down[:, cols], shaped)
     fades = fade.shape[0]
-    noted = note.shape[2]
-    note[s, t] = jnp.concatenate(
+    noted = note.shape[1]
+    note[me] = jnp.concatenate(
         [low, fade[...], jnp.zeros((noted - rank - fades, rows), F32)], axis=0
     )
 
     def note_send(n):
         place, core = (0 if n < tp else last), lax.rem(t + n % tp, tp)
-        ref = note.at[s, t]
-        return remote(ref, ref, n_send.at[n], n_recv.at[s, t], sp=place, tp=core), jnp.logical_or(
-            s != place, core != t
-        )
+        ref = note.at[me]
+        return remote(ref, ref, n_send, n_recv, sp=place, tp=core), (s != place) | (core != t)
 
     for n in range(2 * tp):
         send, away_from_here = note_send(n)
@@ -393,7 +403,7 @@
         src = lin_own.at[b, 1 - way, i, cut] if i < mine else win_own.at[b, 1 - way, cut]
         dst = lin_in.at[way, b, i, cut] if i < mine else win_in.at[way, b, cut]
         return remote(
-            src, dst, r_send.at[way, b, n], r_recv.at[way, b, n], sp=jnp.clip(s + 1 - 2 * way, 0, last)
+            src, dst, r_send.at[0 if i < mine else 1], r_recv.at[way, b, n], sp=jnp.clip(s + 1 - 2 * way, 0, last)
         )
 
     def relay(way, b, n):
@@ -419,11 +429,13 @@
             step(e, b, n).start()
 
     def project(k, carry):
-        b = lax.rem(s + k, sp)
-
-        @pl.when((s > 1) & inside & (k == sp - 1))
-        def _():
-            relay(e, 0, 0)
+        turned = lax.rem(s + k, sp)
+        b = jnp.where(inside & (k > 1), jnp.where(k == 2, 0, sp + 1 - 2 * s), turned)
+
+        @pl.when(inside & (k == last))
+        def _():
+            for n in range(EARLY):
+                relay(e, 0, n)
 
         @pl.when(jnp.logical_or(jnp.logical_not(home), b != s))
         def _():
@@ -437,10 +449,9 @@
         def _():
             keep(0).wait()
 
-        @pl.when(b != s)
-        def _():
-            for pt in range(tp):
-                squares_wait(b, pt)
+        @pl.when(k == 1)
+        def _():
+            squares_wait((sp - 1) * tp, 1)
 
         for i in reversed(range(per_half)):
 
@@ -507,7 +518,7 @@
         i, r = divmod(n, CUTS)
         ref = (held_n if i else held_g).at[b, way, slice(r * cut_rows, (r + 1) * cut_rows)]
         return remote(
-            ref, ref, g_send.at[way, b, n], g_recv.at[way, b, n], sp=jnp.clip(s + 1 - 2 * way, 0, last)
+            ref, ref, g_send.at[i], g_recv.at[way, b, n], sp=jnp.clip(s + 1 - 2 * way, 0, last)
         )
 
     part_rows = rows // tp
@@ -516,8 +527,13 @@
     def swap(b):
         return remote(term.at[b, other], away.at[b], t_send.at[b], t_recv.at[b], tp=other)
 
+    columns = term.shape[3]
+
+    def place_of(src):
+        return pl.ds(pl.multiple_of(src * columns, columns), columns)
+
     def deliver(b):
-        return remote(term.at[b, t], landed.at[s], o_send.at[b], o_recv.at[s], sp=b)
+        return remote(term.at[b, t], out.at[:, place_of(s)], o_send, o_recv, sp=b)
 
     def close(b):
         swap(b).wait()
@@ -529,7 +545,7 @@
 
         @pl.when(s == b)
         def _():
-            landed[b] = term[b, t]
+            out[:, b * columns : (b + 1) * columns] = term[b, t]
 
     def multiply(b):
         total = None
@@ -552,13 +568,7 @@
         items = [(relay, b, i) for b in range(sp) for i in range(len(pieces))]
         items += [(pass_on, b, i) for b in range(sp) for i in range(2 * CUTS)]
         for n in range(len(items) + LAG):
-            if n == 0:
-
-                @pl.when(s <= 1)
-                def _():
-                    relay(e, 0, 0)
-
-            elif n < len(items):
+            if EARLY <= n < len(items):
                 what, b, i = items[n]
                 what(e, b, i)
             if n >= LAG:
@@ -578,14 +588,8 @@
     @pl.when(at_end)
     def _():
         loads[8].wait()
-        for ps in range(sp):
-            for pt in range(tp):
-
-                @pl.when(jnp.logical_or(s != ps, t != pt))
-                def _():
-                    ref = note.at[ps, pt]
-                    remote(ref, ref, n_send.at[0], n_recv.at[ps, pt], tp=other).wait_recv()
-
+        others = note.at[pl.ds(0, sp * tp - 1)]
+        remote(others, others, n_send, n_recv, tp=other).wait_recv()
         span = mine * lk
         lane = pl.ds(pl.multiple_of(e * span, span), span)
         up_own = jnp.concatenate([up[:, lane], jnp.zeros((rows - rank, span), BF)], axis=0)
@@ -602,9 +606,9 @@
         heads = qw // HD // mine
 
         def linear(b, states):
-            rank_rows = note[b, 0, :rank] + note[b, 1, :rank]
+            rank_rows = note[b * tp, :rank] + note[b * tp + 1, :rank]
             tall = jnp.concatenate(
-                [rank_rows, note[b, t, rank:], jnp.zeros((rows - noted, rows), F32)], axis=0
+                [rank_rows, note[b * tp + t, rank:], jnp.zeros((rows - noted, rows), F32)], axis=0
             ).T
             energies = dot(tall.astype(BF), up_own) + bias_own
             soft = jnp.minimum(energies, 0.0) - jnp.log1p(jnp.exp(-jnp.abs(energies)))
@@ -706,61 +710,37 @@
                     close(c)
         close(last)
 
-    def drain(b, carry):
-        for i in range(len(pieces)):
-            for way in range(2):
-
-                @pl.when(s != last * (1 - way))
-                def _():
-                    step(way, b, i).wait_send()
-
-        for i in range(2 * CUTS):
-            for way in range(2):
-
-                @pl.when(s != last * (1 - way))
-                def _():
-                    gather(way, b, i).wait_send()
-
-        @pl.when(home)
-        def _():
-            forward(b).wait_send()
-
-        return carry
-
-    lax.fori_loop(0, sp, drain, 0)
+    def drain(ref, sem):
+        remote(ref, ref, sem, l_sem, tp=other).wait_send()
+
+    sent = ((lin_own, r_send.at[0]), (win_own, r_send.at[1]), (held_g, g_send.at[0]), (held_n, g_send.at[1]))
+
+    @pl.when(inside)
+    def _():
+        for ref, sem in sent:
+            drain(ref, sem)
+        drain(note.at[pl.ds(0, 2 * tp)], n_send)
+
+    @pl.when(at_end)
+    def _():
+        for ref, sem in sent:
+            drain(ref.at[:, 0], sem)
+        drain(note.at[pl.ds(0, 2 * tp - 1)], n_send)
+
+    @pl.when(home)
+    def _():
+        drain(blocks, f_send)
+
     for i in range(per_half):
 
         @pl.when((t * per_half + i != s) & ((s > 0) | (t == 0) | (i < per_half - 1)))
         def _():
             slice_send(i).wait_send()
 
-    for n in range(2 * tp):
-        send, away_from_here = note_send(n)
-
-        @pl.when(away_from_here)
-        def _():
-            send.wait_send()
-
-    for n in range(1, sp * tp):
-        squares_send(n).wait_send()
-
-    columns = landed.shape[2]
-
-    def leave(b):
-        return pltpu.make_async_copy(
-            landed.at[b], out.at[:, pl.ds(b * columns, columns)], y_sem.at[b]
-        )
-
-    for b in range(sp):
-
-        @pl.when(s != b)
-        def _():
-            deliver(b).wait_send()
-            remote(landed.at[b], landed.at[b], o_send.at[b], o_recv.at[b], tp=other).wait_recv()
-
-        leave(b).start()
-    for b in range(sp):
-        leave(b).wait()
+    drain(squares.at[pl.ds(0, sp * tp - 1)], sq_send)
+    drain(term.at[pl.ds(0, last), 0], o_send)
+    others = out.at[:, pl.ds(0, last * columns)]
+    remote(others, others, o_send, o_recv, tp=other).wait_recv()
 
 
 def stationary(
@@ -799,6 +779,14 @@
     mine = heads_tp // 2
     noted = rank + heads_tp + -(rank + heads_tp) % 8
     columns = window_output_weight.shape[1]
+    small = (
+        input_norm_gain.reshape(tp, 1, half),
+        decay_offset_bias.reshape(1, -1),
+        head_sink_logit,
+        linear_head_gain.reshape(1, -1),
+        decay_up_factor,
+        extra_fading_exponent.T,
+    )
     vmem = pl.BlockSpec(memory_space=pltpu.VMEM)
     hbm = pl.BlockSpec(memory_space=pltpu.HBM)
     dma = pltpu.SemaphoreType.DMA
@@ -807,22 +795,18 @@
     win_cols = sum(m.shape[1] for m in matrices[:3]) // 2
     return pl.pallas_call(
         functools.partial(mixer_kernel, sp, tp),
-        out_shape=jax.ShapeDtypeStruct((rows // tp, columns * sp), BF),
-        in_specs=[vmem] * 2
-        + [pl.BlockSpec(memory_space=pltpu.SMEM)]
-        + [vmem] * 3
-        + [hbm] * 11,
-        out_specs=hbm,
+        out_shape=pltpu.VMEM((rows // tp, columns * sp), BF),
+        in_specs=[hbm] * 17,
+        out_specs=vmem,
         scratch_shapes=[pltpu.VMEM(m.shape, BF) for m in matrices]
         + [
             pltpu.VMEM((mine,) + starting_state.shape[1:], F32),
             pltpu.VMEM((rank, half), BF),
             pltpu.VMEM((rows, half), BF),
-            pltpu.VMEM((sp, tp, 8, rows), F32),
+            pltpu.VMEM((sp * tp, 8, rows), F32),
             pltpu.VMEM((sp, rows, slice_width), BF),
-            pltpu.VMEM((sp, tp, noted, rows), F32),
+            pltpu.VMEM((sp * tp, noted, rows), F32),
             pltpu.VMEM((sp, tp, rows // tp, columns), BF),
-            pltpu.VMEM((sp, rows // tp, columns), BF),
             pltpu.VMEM((sp, rows // tp, columns), BF),
             pltpu.VMEM((sp, 2, mine, rows, lin_cols), BF),
             pltpu.VMEM((sp, 2, rows, win_cols), BF),
@@ -831,29 +815,33 @@
             pltpu.VMEM((sp, 2, rows, linear_output_weight.shape[0] // 2), BF),
             pltpu.VMEM((sp, 2, rows, window_output_weight.shape[0] // 2), BF),
             dma((11,)),
-            dma((sp * tp,)),
-            dma((sp, tp)),
+            dma,
+            dma((2,)),
             dma((sp // tp,)),
+            dma((sp,)),
+            dma,
+            dma,
+            dma,
+            dma,
+            dma((2,)),
+            dma((2, sp, (mine + 1) * CUTS)),
+            dma((2,)),
+            dma((2, sp, 2 * CUTS)),
             dma((sp,)),
             dma((sp,)),
             dma,
-            dma((2 * tp,)),
-            dma((sp, tp)),
+            dma,
+            pltpu.SemaphoreType.REGULAR,
+            dma((len(small),)),
         ]
-        + [dma((2, sp, (mine + 1) * CUTS))] * 2
-        + [dma((2, sp, 2 * CUTS))] * 2
-        + [dma((sp,))] * 5
-        + [pltpu.SemaphoreType.REGULAR],
+        + [
+            (pltpu.SMEM if a.ndim == 1 else pltpu.VMEM)(a.shape, a.dtype) for a in small
+        ],
         compiler_params=pltpu.CompilerParams(
             collective_id=0, has_side_effects=True, vmem_limit_bytes=56 * 2**20
         ),
     )(
-        input_norm_gain.reshape(tp, 1, half),
-        decay_offset_bias.reshape(1, -1),
-        head_sink_logit,
-        linear_head_gain.reshape(1, -1),
-        decay_up_factor,
-        extra_fading_exponent.T,
+        *small,
         *matrices,
         starting_state,
         decay_down_factor.T,
@@ -865,7 +853,7 @@
     sp, tp = lax.axis_size("sp"), lax.axis_size("tp")
     rows = arrays[0].shape[0]
     one_each = KVH == GATED_MIXERS == sp * tp and QH % KVH == 0
-    if tp == 2 and sp % tp == 0 and sp > 2 and one_each and rows == WINDOW and rows % SPAN == 0:
+    if tp == 2 and sp == 2 * tp and one_each and rows == WINDOW and rows % SPAN == 0:
         return stationary(*arrays)
     return local(*arrays)
 

time: 104 us -> 98.7 us (0.949)
  Pallas kernels: 101 us -> 97.7 us
  local copies, waits for them, and re-layouts: 1.87 us -> 0.8 us
    pallas_call x1, Pallas kernels: 101 us -> 97.7 us  [stationary(): pl.pallas_call(functools.partial(mixer_kernel, sp, tp), out_shape=pltpu.V...]
    unnamed x1, local copies, waits for them, and re-layouts: 1.87 us -> 0.8 us
where the time goes in v4:
time: 98.7 us; the launch traced here: 98.5 us
  Pallas kernels  97.7 us (99%)
    pallas_call x1, Pallas kernels, stationary(): pl.pallas_call(functools.partial(mixer_kernel, sp, tp), out_shape=pltpu.V...  97.7 us

profile of v4, /device:TPU:0, one launch (start us, length us, event | category | flops | bytes accessed | tf_op | source)
XLA Modules:
  0.0 98.5 jit_solution(17800495478479863481)
XLA Ops:
  0.0 97.7 %shard_map.163 = bf16[64,4096]{1,0:T(8,128)(2,1)S(1)} custom-call(f32[2,1,2048]{2,1,0:T(1,128)} %bitcast.6, f32[1,512]{1,0:T(1,128)} %bitcast.7, f32[16]{0:T(128)} %refs_2_.1, f32[1,256]{1,0:T(1,128)} %bitcast.9, bf16[16,512]{1,0:T(8,128)(2,1)} %refs_4_.1, f32[4,128]{1,0:T(4,128)} %bitcast.8, bf16[1024,1024]{1,0:T(8,128)(2,1)} %refs_6_.1, ...), custom_call_target="tpu_custom_call" | custom-call | tf_op jit(solution)/shard_map/pallas_call | solution.py:796
  97.7 0.8 copy.19

commit v5 on v4

--- a/solution.py
+++ b/solution.py
@@ -279,11 +279,11 @@
     small_in, sources, state_in, down_in, x_in = refs[:6], refs[6:14], refs[14], refs[15], refs[16]
     out = refs[17]
     weights, start, down, x = refs[18:26], refs[26], refs[27], refs[28]
-    gain, bias, sink, head_gain, up, fade = refs[59:65]
+    gain, bias, sink, head_gain, up, fade = refs[58:64]
     squares, blocks, note, term, away = refs[29:34]
     lin_own, win_own, lin_in, win_in, held_g, held_n = refs[34:40]
     w_sem, sq_send, sq_recv, a_send, a_recv, f_send, l_sem, n_send, n_recv = refs[40:49]
-    r_send, r_recv, g_send, g_recv, t_send, t_recv, o_send, o_recv, turn, s_sem = refs[49:59]
+    r_send, r_recv, g_send, g_recv, t_send, t_recv, o_send, o_recv, s_sem = refs[49:58]
     s, t = lax.axis_index("sp"), lax.axis_index("tp")
     other = 1 - t
     last = sp - 1
@@ -309,7 +309,7 @@
     )
     loads.append(pltpu.make_async_copy(x_in, x, w_sem.at[10]))
     small = [
-        pltpu.make_async_copy(a, b, s_sem.at[i]) for i, (a, b) in enumerate(zip(small_in, refs[59:65]))
+        pltpu.make_async_copy(a, b, s_sem.at[i]) for i, (a, b) in enumerate(zip(small_in, refs[58:64]))
     ]
     loads[10].start()
     for copy in small:
@@ -388,13 +388,6 @@
         ref = note.at[me]
         return remote(ref, ref, n_send, n_recv, sp=place, tp=core), (s != place) | (core != t)
 
-    for n in range(2 * tp):
-        send, away_from_here = note_send(n)
-
-        @pl.when(away_from_here)
-        def _():
-            send.start()
-
     cut_rows = rows // CUTS
     pieces = [(i, slice(r * cut_rows, (r + 1) * cut_rows)) for i in range(mine + 1) for r in range(CUTS)]
 
@@ -434,7 +427,7 @@
 
         @pl.when(inside & (k == last))
         def _():
-            for n in range(EARLY):
+            for n in range(1, EARLY):
                 relay(e, 0, n)
 
         @pl.when(jnp.logical_or(jnp.logical_not(home), b != s))
@@ -474,14 +467,8 @@
                 lin_own[b, h, i, :, 2 * lk :] = value[:, i * DV : (i + 1) * DV]
             if n == 0:
 
-                @pl.when((s == 0) & (t > 0) & (k == 0))
-                def _():
-                    slice_send(per_half - 1).wait_send()
-                    pl.semaphore_signal(turn, inc=1, device_id={"tp": other}, device_id_type=MESH)
-
                 @pl.when((s == 0) & (t == 0) & (k == 0))
                 def _():
-                    pl.semaphore_wait(turn, 1)
                     for i in range(1, per_half):
                         slice_send(i).start()
 
@@ -496,10 +483,25 @@
                     for m in range(mine * CUTS):
                         step(e, b, m).start()
 
+            if n == 0:
+
+                @pl.when(k == 0)
+                def _():
+                    for m in range(2 * tp):
+                        send, away_from_here = note_send(m)
+
+                        @pl.when(away_from_here)
+                        def _():
+                            send.start()
+
             win_own[b, h, :, :qw] = part(0, h)
             win_own[b, h, :, qw : qw + kw] = part(1, h)
             win_own[b, h, :, qw + kw :] = part(2, h)
             if n == 0:
+
+                @pl.when(inside & (k == 2))
+                def _():
+                    relay(e, 0, 0)
 
                 @pl.when(at_end & (k >= e))
                 def _():
@@ -733,7 +735,7 @@
 
     for i in range(per_half):
 
-        @pl.when((t * per_half + i != s) & ((s > 0) | (t == 0) | (i < per_half - 1)))
+        @pl.when(t * per_half + i != s)
         def _():
             slice_send(i).wait_send()
 
@@ -831,7 +833,6 @@
             dma((sp,)),
             dma,
             dma,
-            pltpu.SemaphoreType.REGULAR,
             dma((len(small),)),
         ]
         + [

time: 98.7 us -> 97.8 us (level)
  no operation moved by 1% of the time
where the time goes in v5:
time: 97.8 us; the launch traced here: 97.7 us
  Pallas kernels  96.9 us (99%)
    pallas_call x1, Pallas kernels, stationary(): pl.pallas_call(functools.partial(mixer_kernel, sp, tp), out_shape=pltpu.V...  96.9 us

profile of v5, /device:TPU:0, one launch (start us, length us, event | category | flops | bytes accessed | tf_op | source)
XLA Modules:
  0.0 97.7 jit_solution(16959267431237960435)
XLA Ops:
  0.0 96.9 %shard_map.163 = bf16[64,4096]{1,0:T(8,128)(2,1)S(1)} custom-call(f32[2,1,2048]{2,1,0:T(1,128)} %bitcast.6, f32[1,512]{1,0:T(1,128)} %bitcast.7, f32[16]{0:T(128)} %refs_2_.1, f32[1,256]{1,0:T(1,128)} %bitcast.9, bf16[16,512]{1,0:T(8,128)(2,1)} %refs_4_.1, f32[4,128]{1,0:T(4,128)} %bitcast.8, bf16[1024,1024]{1,0:T(8,128)(2,1)} %refs_6_.1, ...), custom_call_target="tpu_custom_call" | custom-call | tf_op jit(solution)/shard_map/pallas_call | solution.py:798
  96.9 0.8 copy.19

commit v6 on v5

--- a/solution.py
+++ b/solution.py
@@ -349,7 +349,7 @@
     for i in reversed(range(per_half)):
         j = t * per_half + i
 
-        @pl.when((j < s) | ((j > s) & (s == 0) & (t > 0)))
+        @pl.when(((j < s) & ((s < last) | (t == 0))) | ((j > s) & (s == 0) & (t > 0)))
         def _():
             slice_send(i).start()
 
@@ -466,6 +466,11 @@
                 lin_own[b, h, i, :, lk : 2 * lk] = key[:, i * lk : (i + 1) * lk]
                 lin_own[b, h, i, :, 2 * lk :] = value[:, i * DV : (i + 1) * DV]
             if n == 0:
+
+                @pl.when((s == last) & (t > 0) & (k == 0))
+                def _():
+                    for i in range(per_half - 1):
+                        slice_send(i).start()
 
                 @pl.when((s == 0) & (t == 0) & (k == 0))
                 def _():
@@ -583,9 +588,18 @@
                     if b == last:
                         for c in range(1, last):
                             close(c)
+
+                        @pl.when(s == 1)
+                        def _():
+                            close(0)
+
                     multiply(b)
         close(last)
-        close(0)
+
+        @pl.when(s > 1)
+        def _():
+            close(0)
+
 
     @pl.when(at_end)
     def _():

time: 97.8 us -> 97.7 us (level)
  no operation moved by 1% of the time
where the time goes in v6:
time: 97.7 us; the launch traced here: 97.5 us
  Pallas kernels  96.7 us (99%)
    pallas_call x1, Pallas kernels, stationary(): pl.pallas_call(functools.partial(mixer_kernel, sp, tp), out_shape=pltpu.V...  96.7 us

profile of v6, /device:TPU:0, one launch (start us, length us, event | category | flops | bytes accessed | tf_op | source)
XLA Modules:
  0.0 97.5 jit_solution(11250286017824744494)
XLA Ops:
  0.0 96.7 %shard_map.163 = bf16[64,4096]{1,0:T(8,128)(2,1)S(1)} custom-call(f32[2,1,2048]{2,1,0:T(1,128)} %bitcast.6, f32[1,512]{1,0:T(1,128)} %bitcast.7, f32[16]{0:T(128)} %refs_2_.1, f32[1,256]{1,0:T(1,128)} %bitcast.9, bf16[16,512]{1,0:T(8,128)(2,1)} %refs_4_.1, f32[4,128]{1,0:T(4,128)} %bitcast.8, bf16[1024,1024]{1,0:T(8,128)(2,1)} %refs_6_.1, ...), custom_call_target="tpu_custom_call" | custom-call | tf_op jit(solution)/shard_map/pallas_call | solution.py:812
  96.7 0.8 copy.19
